TPU v7x, 32 devices: a whole 2x2x4 slice. The times are simulated.
32 devices in a mesh: grp: 2 (over y), fs: 4 (over z), tp: 4 (over x, core).
Axes of the slice: x: 2, y: 2, z: 4, core: 2. Of those that a mesh axis runs over, the one named last changes fastest.
Arguments:
- tokens: bfloat16 [4096, 2048], P(('grp', 'tp')), parts along dimension 0, may hold values from -6 to 6
- gate_weight: float32 [2, 2048, 5632], P(None, 'fs', 'tp'), may hold values from -0.125 to 0.125
- up_weight: float32 [2, 2048, 5632], P(None, 'fs', 'tp'), may hold values from -0.125 to 0.125
- down_weight: float32 [2, 2048, 5632], P(None, 'fs', 'tp'), may hold values from -0.078125 to 0.078125
- in_gain: float32 [2, 2048], P(None, 'fs'), may hold values from 0.1 to 1.9
- out_gain: float32 [2, 2048], replicated, may hold values from 0.1 to 1.9
Outputs:
- sampler_gate: bfloat16 [4, 2048, 5632], P('grp', None, 'fs'), parts along dimension 0
- sampler_up: bfloat16 [4, 2048, 5632], P('grp', None, 'fs'), parts along dimension 0
- sampler_down: bfloat16 [4, 2048, 5632], P('grp', None, 'fs'), parts along dimension 0
- result: bfloat16 [4096, 2048], P(('grp', 'tp', 'fs')), parts along dimension 0
There are 2 independent parts, one for each index of `grp`. A program takes and returns all parts, laid end to end along the dimension named above; an argument that names none is the same for every part. Nothing has to cross between parts.
All inputs are finite; a program needn't handle non-finite values.
Results may differ from a plain program's by a relative error of at most 0.0073.
Values may be sent and summed in bfloat16 or wider, within the bound.
A program may use at most 192 MiB of HBM per device.

v0:
```python
import functools

import jax
import jax.numpy as jnp
from jax import lax
from jax.experimental import pallas as pl
from jax.experimental.pallas import tpu as pltpu
from jax.sharding import PartitionSpec as P

EPS = 1e-06


def normalize(rows):
    return rows * lax.rsqrt(jnp.mean(rows * rows, axis=-1, keepdims=True) + EPS)


def body_plain(tokens, gate_weight, up_weight, down_weight, in_gain, out_gain):
    groups = lax.axis_size("fs")
    rows_all = tokens.shape[0]
    rows_mine = rows_all // groups
    model_width = tokens.shape[1]
    local_rows = gate_weight.shape[1]
    block_width = gate_weight.shape[2] // groups
    residual = lax.dynamic_slice_in_dim(
        tokens, lax.axis_index("fs") * rows_mine, rows_mine, 0
    ).astype(jnp.float32)
    normed = normalize(tokens.astype(jnp.float32)).astype(jnp.bfloat16)
    gates = []
    ups = []
    downs = []
    rounded_state = tokens
    contract_last = (((1,), (1,)), ((), ()))
    for section_idx in range(2):
        scale = in_gain[section_idx][:, None]
        gate_rounded = (scale * gate_weight[section_idx]).astype(jnp.bfloat16)
        up_rounded = (scale * up_weight[section_idx]).astype(jnp.bfloat16)
        down_rounded = down_weight[section_idx].astype(jnp.bfloat16)
        flipped = [
            w.T.reshape(groups, block_width, local_rows)
            for w in (gate_rounded, up_rounded, down_rounded)
        ]
        arrived = (
            lax.all_to_all(flipped[0], "fs", split_axis=0, concat_axis=2, tiled=True),
            lax.all_to_all(flipped[1], "fs", split_axis=0, concat_axis=2, tiled=True),
            lax.all_to_all(flipped[2], "fs", split_axis=0, concat_axis=2, tiled=True),
        )
        thin_rows = [w.reshape(block_width, model_width) for w in arrived]
        sampler_mats = (
            lax.all_gather(thin_rows[0], "tp", axis=0, tiled=True),
            lax.all_gather(thin_rows[1], "tp", axis=0, tiled=True),
            lax.all_gather(thin_rows[2], "tp", axis=0, tiled=True),
        )
        gate_flip, up_flip, down_flip = (sampler_mats[0], sampler_mats[1], sampler_mats[2])
        gates.append(gate_flip.T)
        ups.append(up_flip.T)
        downs.append(down_flip.T)

        def hidden_of(row_block):
            gate_act = lax.dot_general(
                row_block, gate_flip, contract_last, preferred_element_type=jnp.float32
            )
            up_act = lax.dot_general(
                row_block, up_flip, contract_last, preferred_element_type=jnp.float32
            )
            return (jax.nn.silu(gate_act) * up_act).astype(jnp.bfloat16)

        if section_idx == 0:
            hidden = hidden_of(normed)
        else:
            hidden = hidden_of(lax.all_gather(normed, "fs", axis=0, tiled=True))
        mixed = lax.psum_scatter(
            jnp.dot(hidden, down_flip, preferred_element_type=jnp.float32),
            "fs",
            scatter_dimension=0,
            tiled=True,
        )
        rounded_state = (residual + 0.5 * out_gain[section_idx] * normalize(mixed)).astype(
            jnp.bfloat16
        )
        if section_idx == 0:
            residual = rounded_state.astype(jnp.float32)
            normed = normalize(residual).astype(jnp.bfloat16)
    return (jnp.stack(gates), jnp.stack(ups), jnp.stack(downs), rounded_state)


def prep_kernel(blocks, width, part, scaled, where, *refs):
    if scaled:
        gain, weight, out, flip = refs
        rows = weight[0] * gain[0]
    else:
        weight, out, flip = refs
        rows = weight[0]
    flip[...] = rows.astype(jnp.bfloat16).T
    skip = where[0] * part if part < width else 0
    for target in range(blocks):
        start = pl.multiple_of(target * width + skip, 16)
        out[target] = flip[pl.ds(start, part), :]


def prepare(where, weight, gain, layer, blocks, halves):
    _, rows, cols = weight.shape
    width = cols // blocks
    part = width // halves
    step = 256 if rows % 256 == 0 else rows
    in_specs = [pl.BlockSpec((1, step, cols), lambda r, where: (layer, r, 0))]
    args = [weight]
    if gain is not None:
        in_specs.insert(0, pl.BlockSpec((1, step, 1), lambda r, where: (layer, r, 0)))
        args.insert(0, gain)
    return pl.pallas_call(
        functools.partial(prep_kernel, blocks, width, part, gain is not None),
        grid_spec=pltpu.PrefetchScalarGridSpec(
            num_scalar_prefetch=1,
            grid=(rows // step,),
            in_specs=in_specs,
            out_specs=pl.BlockSpec((blocks, part, step), lambda r, where: (0, 0, r)),
            scratch_shapes=[pltpu.VMEM((cols, step), jnp.bfloat16)],
        ),
        out_shape=jax.ShapeDtypeStruct((blocks, part, rows), jnp.bfloat16),
        cost_estimate=pl.CostEstimate(
            flops=rows * cols, bytes_accessed=rows * cols * 5, transcendentals=0
        ),
    )(where, *args)


def spread_kernel(blocks, split, *refs):
    n = len(split)
    sources, full = refs[:n], refs[n : 2 * n]
    own, (own_sem, send_sem, recv_sem) = refs[2 * n : 3 * n], refs[3 * n :]
    y, z, t = lax.axis_index("grp"), lax.axis_index("fs"), lax.axis_index("tp")
    x, c = t // 2, lax.rem(t, 2)
    other_y, other_x, other_c = 1 - y, (1 - x) * 2 + c, x * 2 + (1 - c)
    wide = sources[0].shape[-1]
    partners = [{"fs": lax.rem(z + shift, blocks)} for shift in range(1, blocks)]
    partners += [{"tp": other_x}, {"tp": other_c}, {"grp": other_y}]

    barrier = pltpu.get_barrier_semaphore()
    for partner in partners:
        pl.semaphore_signal(barrier, inc=1, device_id=partner, device_id_type=pl.DeviceIdType.MESH)
    pl.semaphore_wait(barrier, len(partners))

    def columns(source):
        return pl.ds(pl.multiple_of(source * wide, 128), wide)

    def place(m, column, half, source):
        cols = columns(source)
        if not split[m]:
            return full[m].at[column, :, :, cols]
        return full[m].at[column, half, :, cols]

    def rows_of(m, column, half):
        if not split[m]:
            return full[m].at[column]
        return full[m].at[column, half]

    def origin(m, target):
        return sources[m].at[target]

    names = []
    sent = []

    def slot(name):
        if name not in names:
            names.append(name)
        return names.index(name)

    def send(name, source, target, device):
        k = slot(name)
        copy = pltpu.make_async_remote_copy(
            src_ref=source,
            dst_ref=target,
            send_sem=send_sem.at[k],
            recv_sem=recv_sem.at[k],
            device_id=device,
            device_id_type=pl.DeviceIdType.MESH,
        )
        copy.start()
        sent.append(copy)

    def arrived(name, landed, device):
        k = slot(name)
        pltpu.make_async_remote_copy(
            src_ref=landed,
            dst_ref=landed,
            send_sem=send_sem.at[k],
            recv_sem=recv_sem.at[k],
            device_id=device,
            device_id_type=pl.DeviceIdType.MESH,
        ).wait_recv()

    to_x, to_c, to_y = {"tp": other_x}, {"tp": other_c}, {"grp": other_y}
    fetch = []
    for m in range(n):
        for shift in range(1, blocks):
            target = lax.rem(z + shift, blocks)
            send(("z", m, shift), origin(m, target), place(m, t, y, z), {"fs": target})
        mine = origin(m, z)
        send(("x", m, 0), mine, place(m, t, y, z), to_x)
        if split[m]:
            send(("y", m, 0, 0), mine, place(m, t, y, z), to_y)
        copy = pltpu.make_async_copy(mine, own[m], own_sem.at[m])
        copy.start()
        fetch.append(copy)
    kept = []
    for m in range(n):
        fetch[m].wait()
        copy = pltpu.make_async_copy(own[m], place(m, t, y, z), own_sem.at[n + m])
        copy.start()
        kept.append(copy)

    def relay(m, shift):
        source = lax.rem(z + blocks - shift, blocks)
        arrived(("x", m, shift), place(m, other_x, y, source), to_x)
        if split[m]:
            spot = place(m, other_x, y, source)
            send(("y", m, 1, shift), spot, spot, to_y)

    for m in range(n):
        for shift in range(1, blocks):
            source = lax.rem(z + blocks - shift, blocks)
            spot = place(m, t, y, source)
            arrived(("z", m, shift), spot, {"fs": source})
            send(("x", m, shift), spot, spot, to_x)
            if split[m]:
                send(("y", m, 0, shift), spot, spot, to_y)
            relay(m, shift - 1)
        kept[m].wait()
        send(("c", m, 0, 0), rows_of(m, t, y), rows_of(m, t, y), to_c)
        relay(m, blocks - 1)
        send(("c", m, 1, 0), rows_of(m, other_x, y), rows_of(m, other_x, y), to_c)
    for m in range(n):
        if not split[m]:
            continue
        for far, column in ((0, t), (1, other_x)):
            for shift in range(blocks):
                source = lax.rem(z + blocks - shift, blocks)
                arrived(("y", m, far, shift), place(m, column, other_y, source), to_y)
            rows = rows_of(m, column, other_y)
            send(("c", m, far, 1), rows, rows, to_c)
    other_both = (1 - x) * 2 + (1 - c)
    for m in range(n):
        for far, column in ((0, other_c), (1, other_both)):
            arrived(("c", m, far, 0), rows_of(m, column, y), to_c)
            if split[m]:
                arrived(("c", m, far, 1), rows_of(m, column, other_y), to_c)
    for copy in sent:
        copy.wait_send()


def spread(sources, split, blocks, columns):
    n, halves = len(split), 2
    part, rows = sources[0].shape[1:]
    sources = [
        source if alone else source.reshape(blocks, halves, part, rows)
        for source, alone in zip(sources, split)
    ]
    count = sum(4 * blocks + 1 + (2 * blocks + 2) * alone for alone in split)
    shape = (columns, halves, part, rows * blocks)
    moved = n * columns * halves * part * rows * blocks * 2
    whole = pl.BlockSpec(memory_space=pl.ANY)
    return pl.pallas_call(
        functools.partial(spread_kernel, blocks, split),
        in_specs=[whole] * n,
        out_specs=[whole] * n,
        out_shape=[jax.ShapeDtypeStruct(shape, jnp.bfloat16)] * n,
        scratch_shapes=[pltpu.VMEM(source.shape[1:], jnp.bfloat16) for source in sources]
        + [
            pltpu.SemaphoreType.DMA((2 * n,)),
            pltpu.SemaphoreType.DMA((count,)),
            pltpu.SemaphoreType.DMA((count,)),
        ],
        compiler_params=pltpu.CompilerParams(collective_id=0, has_side_effects=True),
        cost_estimate=pl.CostEstimate(flops=0, bytes_accessed=moved * 13, transcendentals=0),
    )(*sources)


def emit_kernel(flip, *refs):
    refs[-1][0] = flip[...].T


def emit(flip, layer, stacked):
    hidden, width = flip.shape
    step = 256
    in_specs = [pl.BlockSpec((hidden, step), lambda r: (0, r))]
    args = [flip]
    aliases = {}
    if stacked is not None:
        in_specs.append(pl.BlockSpec(memory_space=pl.ANY))
        args.append(stacked)
        aliases = {1: 0}
    return pl.pallas_call(
        emit_kernel,
        grid=(width // step,),
        in_specs=in_specs,
        out_specs=pl.BlockSpec((1, step, hidden), lambda r: (layer, r, 0)),
        out_shape=jax.ShapeDtypeStruct((2, width, hidden), jnp.bfloat16),
        input_output_aliases=aliases,
        cost_estimate=pl.CostEstimate(
            flops=0, bytes_accessed=4 * hidden * width, transcendentals=0
        ),
    )(*args)


def body(tokens, gate_weight, up_weight, down_weight, in_gain, out_gain):
    groups = lax.axis_size("fs")
    halves = lax.axis_size("grp")
    block_width = gate_weight.shape[2] // groups
    model_width = tokens.shape[1]
    columns = lax.axis_size("tp")
    odd = block_width % 32 or gate_weight.shape[1] % 128 or gate_weight.shape[2] % 128
    if odd or model_width % 256 or halves != 2 or columns != 4:
        return body_plain(tokens, gate_weight, up_weight, down_weight, in_gain, out_gain)
    rows_mine = tokens.shape[0] // groups
    here = lax.axis_index("fs")
    where = lax.axis_index("grp")[None].astype(jnp.int32)
    gain_column = in_gain[:, :, None]
    contract_last = (((1,), (1,)), ((), ()))
    pieces = [
        [
            prepare(where, gate_weight, gain_column, layer, groups, halves),
            prepare(where, up_weight, gain_column, layer, groups, halves),
            prepare(where, down_weight, None, layer, groups, 1),
        ]
        for layer in range(2)
    ]
    residual = lax.dynamic_slice_in_dim(tokens, here * rows_mine, rows_mine, 0).astype(jnp.float32)
    normed = normalize(tokens.astype(jnp.float32)).astype(jnp.bfloat16)
    order = ((0, 0), (0, 1), (1, 0), (1, 1), (0, 2), (1, 2))
    split = tuple(which < 2 for _, which in order)
    sent = [pieces[layer][which] for layer, which in order]
    whole = dict(zip(order, spread(sent, split, groups, columns)))
    sampler = [
        [whole[layer, which].reshape(columns * block_width, model_width) for which in range(3)]
        for layer in range(2)
    ]
    for layer in range(2):
        flips = sampler[layer]
        gate_flip, up_flip, down_flip = flips
        gate_act = lax.dot_general(normed, gate_flip, contract_last, preferred_element_type=jnp.float32)
        up_act = lax.dot_general(normed, up_flip, contract_last, preferred_element_type=jnp.float32)
        hidden = (jax.nn.silu(gate_act) * up_act).astype(jnp.bfloat16)
        partial = jnp.dot(hidden, down_flip, preferred_element_type=jnp.float32).astype(jnp.bfloat16)
        mixed = lax.psum_scatter(partial, "fs", scatter_dimension=0, tiled=True)
        if layer == 0:
            mixed, first = lax.optimization_barrier((mixed, [emit(flip, 0, None) for flip in flips]))
        mixed = mixed.astype(jnp.float32)
        rounded_state = (residual + 0.5 * out_gain[layer] * normalize(mixed)).astype(jnp.bfloat16)
        if layer == 0:
            residual = rounded_state.astype(jnp.float32)
            normed = normalize(residual).astype(jnp.bfloat16)
            normed, first = lax.optimization_barrier((normed, first))
            normed = lax.all_gather(normed, "fs", axis=0, tiled=True)
            early = emit(sampler[1][0], 1, first[0])
            normed, early = lax.optimization_barrier((normed, early))
            stacked = [early, *first[1:]]
        else:
            stacked[1:] = [emit(flip, 1, held) for flip, held in zip(flips[1:], stacked[1:])]
    return (*stacked, rounded_state)


def solution(mesh):
    in_specs = (
        P(("grp", "tp"), None),
        P(None, "fs", "tp"),
        P(None, "fs", "tp"),
        P(None, "fs", "tp"),
        P(None, "fs"),
        P(),
    )
    out_specs = (
        P("grp", None, "fs"),
        P("grp", None, "fs"),
        P("grp", None, "fs"),
        P(("grp", "tp", "fs"), None),
    )
    return jax.shard_map(body, mesh=mesh, in_specs=in_specs, out_specs=out_specs, check_vma=False)
```

profile of v0, /device:TPU:0, one launch (start us, length us, event | category | flops | bytes accessed | tf_op | source)
XLA Modules:
  0.0 383.6 jit_solution(9476571032807753940)
XLA Ops:
  7.2 0.0 reduce-scatter.3.cloned.1.call-start
  7.2 1.7 copy.13.refs_0_
  8.9 3.0 shard_map.93.refs_0_
  11.9 3.0 shard_map.95.refs_2_
  14.9 3.0 shard_map.94.refs_1_
  17.9 3.0 shard_map.96.refs_3_
  20.9 2.9 shard_map.97
  23.8 0.0 copy-start
  23.8 3.0 shard_map.98
  26.9 0.0 copy-done
  26.9 0.5 fusion
  27.4 165.2 %shard_map.99 = (bf16[4,2,176,2048]{3,2,1,0:T(8,128)(2,1)}, bf16[4,2,176,2048]{3,2,1,0:T(8,128)(2,1)}, bf16[4,2,176,2048]{3,2,1,0:T(8,128)(2,1)}, bf16[4,2,176,2...) custom-call(bf16[4,176,512]{2,1,0:T(8,128)(2,1)} %shard_map.93.refs_0_, ...), custom_call_target="tpu_custom_call" | custom-call | bytes 449839104 | tf_op jit(solution)/shard_map/pallas_call | solution.py:261
  192.6 7.7 %fusion.14 = f32[512,1408]{1,0:T(8,128)} fusion(bf16[1408,2048]{1,0:T(8,128)(2,1)} %bitcast.30, bf16[512,2048]{1,0:T(8,128)(2,1)S(1)} %copy-done, f32[512]{0:T(512)S(1)} %add_rsqrt_fusion), kind=kOutput, calls=%fused_computation.26 | convolution fusion | flops 2955935744 | bytes 10749952 | tf_op jit(solution)/shard_map/dot_general | solution.py:339
  200.2 13.3 %convolution_convert_fusion.1 = bf16[512,2048]{1,0:T(8,128)(2,1)} fusion(bf16[1408,2048]{1,0:T(8,128)(2,1)} %bitcast.26, bf16[1408,2048]{1,0:T(8,128)(2,1)} %bitcast.28, f32[512,1408]{1,0:T(8,128)} %fusion.14, bf16[512,2048]{1,0:T(8,128)(2,1)S(1)} %copy-done, f32[512]{0:T(512)S(1)} %add_rsqrt_fusion), kind=kOutput, calls=%fused_computation.9 | convolution fusion | flops 5914099712 | bytes 18614272 | tf_op jit(solution)/shard_map/dot_general | solution.py:342
  213.6 0.0 reduce-scatter.3.cloned.1.call-update
  213.6 0.2 all-gather.2.cloned.1.call-start
  213.8 8.2 %shard_map.100.refs_0_ = bf16[2,2048,1408]{2,1,0:T(8,128)(2,1)} custom-call(bf16[1408,2048]{1,0:T(8,128)(2,1)} %bitcast.31), custom_call_target="tpu_custom_call" | custom-call | bytes 11534336 | tf_op jit(solution)/shard_map/pallas_call | solution.py:291
  222.1 8.4 %shard_map.101.refs_0_ = bf16[2,2048,1408]{2,1,0:T(8,128)(2,1)} custom-call(bf16[1408,2048]{1,0:T(8,128)(2,1)} %bitcast.29), custom_call_target="tpu_custom_call" | custom-call | bytes 11534336 | tf_op jit(solution)/shard_map/pallas_call | solution.py:291
  230.5 0.0 copy-start.1
  230.5 8.3 %shard_map.102.refs_0_ = bf16[2,2048,1408]{2,1,0:T(8,128)(2,1)} custom-call(bf16[1408,2048]{1,0:T(8,128)(2,1)} %bitcast.27), custom_call_target="tpu_custom_call" | custom-call | bytes 11534336 | tf_op jit(solution)/shard_map/pallas_call | solution.py:291
  238.8 0.0 copy-done.1
  238.8 21.8 %reduce-scatter.3.cloned.1.call-done = bf16[128,2048]{1,0:T(8,128)(2,1)} async-done(((bf16[512,2048]{1,0:T(8,128)(2,1)}), bf16[128,2048]{1,0:T(8,128)(2,1)}) %reduce-scatter.3.cloned.1.call-update) | async-done | bytes 524304 | tf_op jit(solution)/shard_map/reduce_scatter | solution.py:343
  260.6 1.2 fusion.4
  261.8 1.5 fusion.10
  263.3 1.0 fusion.11
  264.2 0.0 all-gather.2.cloned.1.call-update
  264.2 0.0 reduce-scatter.5.cloned.1.call-start
  264.3 8.3 %shard_map.103 = bf16[2,2048,1408]{2,1,0:T(8,128)(2,1)} custom-call(bf16[1408,2048]{1,0:T(8,128)(2,1)} %bitcast.24, bf16[2,2048,1408]{2,1,0:T(8,128)(2,1)} %shard_map.100.refs_0_), custom_call_target="tpu_custom_call", output_to_operand_aliasing={{}: (1, {})} | custom-call | bytes 11534336 | tf_op jit(solution)/shard_map/pallas_call | solution.py:291
  272.6 36.6 %all-gather.2.cloned.1.call-done = bf16[512,2048]{1,0:T(8,128)(2,1)} async-done(((bf16[128,2048]{1,0:T(8,128)(2,1)}), bf16[512,2048]{1,0:T(8,128)(2,1)}) %all-gather.2.cloned.1.call-update) | async-done | bytes 2097168 | tf_op jit(solution)/shard_map/all_gather | solution.py:352
  309.2 0.0 copy-start.2
  309.2 8.4 %fusion.21 = f32[512,1408]{1,0:T(8,128)} fusion(bf16[512,2048]{1,0:T(8,128)(2,1)} %all-gather.2.cloned.1.call-done, bf16[1408,2048]{1,0:T(8,128)(2,1)} %bitcast.25), kind=kOutput, calls=%fused_computation.35 | convolution fusion | flops 2952790016 | bytes 10747904 | tf_op jit(solution)/shard_map/dot_general | solution.py:339
  317.7 0.0 copy-done.2
  317.7 13.4 %convolution_convert_fusion = bf16[512,2048]{1,0:T(8,128)(2,1)} fusion(bf16[1408,2048]{1,0:T(8,128)(2,1)} %bitcast.22, bf16[512,2048]{1,0:T(8,128)(2,1)S(1)} %copy-done.2, bf16[1408,2048]{1,0:T(8,128)(2,1)} %bitcast.20, f32[512,1408]{1,0:T(8,128)} %fusion.21), kind=kOutput, calls=%fused_computation.8 | convolution fusion | flops 5910953984 | bytes 18612224 | tf_op jit(solution)/shard_map/dot_general | solution.py:342
  331.1 0.0 reduce-scatter.5.cloned.1.call-update
  331.1 8.3 %shard_map.105 = bf16[2,2048,1408]{2,1,0:T(8,128)(2,1)} custom-call(bf16[1408,2048]{1,0:T(8,128)(2,1)} %bitcast.23, bf16[2,2048,1408]{2,1,0:T(8,128)(2,1)} %shard_map.102.refs_0_), custom_call_target="tpu_custom_call", output_to_operand_aliasing={{}: (1, {})} | custom-call | bytes 11534336 | tf_op jit(solution)/shard_map/pallas_call | solution.py:291
  339.4 8.3 %shard_map.104 = bf16[2,2048,1408]{2,1,0:T(8,128)(2,1)} custom-call(bf16[1408,2048]{1,0:T(8,128)(2,1)} %bitcast.21, bf16[2,2048,1408]{2,1,0:T(8,128)(2,1)} %shard_map.101.refs_0_), custom_call_target="tpu_custom_call", output_to_operand_aliasing={{}: (1, {})} | custom-call | bytes 11534336 | tf_op jit(solution)/shard_map/pallas_call | solution.py:291
  347.6 26.0 %reduce-scatter.5.cloned.1.call-done = bf16[128,2048]{1,0:T(8,128)(2,1)} async-done(((bf16[512,2048]{1,0:T(8,128)(2,1)}), bf16[128,2048]{1,0:T(8,128)(2,1)}) %reduce-scatter.5.cloned.1.call-update) | async-done | bytes 524304 | tf_op jit(solution)/shard_map/reduce_scatter | solution.py:343
  373.7 1.2 fusion.8
  374.9 2.1 fusion.12
  (5 shorter events, 0.1 us)
Async XLA Ops:
  7.2 253.4 %reduce-scatter.3.cloned.1.call-start = ((), (), s32[]{:S(2)}) async-start(), calls=%async_computation.2 | async-start | bytes 2621440 | tf_op jit(solution)/shard_map/reduce_scatter | solution.py:343
  23.8 3.0 copy-start
  213.6 95.7 %all-gather.2.cloned.1.call-start = ((), (), s32[]{:S(2)}) async-start(), calls=%async_computation.3 | async-start | bytes 2621440 | tf_op jit(solution)/shard_map/all_gather | solution.py:352
  230.5 8.3 %copy-start.1 = (f32[2,2048]{1,0:T(2,128)S(1)}, f32[2,2048]{1,0:T(2,128)}, u32[]{:S(2)}) copy-start(f32[2,2048]{1,0:T(2,128)} %param.11) | copy-start | bytes 49156
  264.2 109.4 %reduce-scatter.5.cloned.1.call-start = ((), (), s32[]{:S(2)}) async-start(), calls=%async_computation.4 | async-start | bytes 2621440 | tf_op jit(solution)/shard_map/reduce_scatter | solution.py:343
  309.2 8.4 %copy-start.2 = (bf16[512,2048]{1,0:T(8,128)(2,1)S(1)}, bf16[512,2048]{1,0:T(8,128)(2,1)}, u32[]{:S(2)}) copy-start(bf16[512,2048]{1,0:T(8,128)(2,1)} %all-gather.2.cloned.1.call-done) | copy-start | bytes 6291460
Sparse Core Ops, SparseCore 0:
  213.7 46.8 reduce-scatter.2
  264.4 44.8 all-gather.1
  331.2 42.4 reduce-scatter.4
where the time goes:
time: 385 us; the launch traced here: 384 us
  Pallas kernels  233 us (61%)
  waiting for transfers between devices  84.5 us (22%)
  matrix products  42.8 us (11%)
  between operations  13.8 us (4%)
  other arithmetic  7.5 us (2%)
    pallas_call x1, Pallas kernels, spread(): pl.pallas_call(functools.partial(spread_kernel, blocks, split), in_specs=...  165 us
    pallas_call x6, Pallas kernels, emit(): pl.pallas_call(emit_kernel, grid=(width // step,), in_specs=in_specs, out...  49.8 us
    reduce_scatter x2, waiting for transfers between devices, body(): mixed = lax.psum_scatter(partial, 'fs', scatter_dimension=0, tiled=True)  47.8 us
    all_gather x1, waiting for transfers between devices, body(): normed = lax.all_gather(normed, 'fs', axis=0, tiled=True)  36.6 us
    dot_general x2, matrix products, body(): jnp.dot(hidden, down_flip, preferred_element_type=jnp.float32)  26.7 us
    pallas_call x6, Pallas kernels, prepare(): pl.pallas_call(functools.partial(prep_kernel, blocks, width, part, gain i...  18 us
    dot_general x2, matrix products, body(): lax.dot_general(normed, gate_flip, contract_last, preferred_element_type=...  16.1 us
  transfers between devices with their start and end apart: 3, of which 3 were waited for; matrix products, arithmetic and copies ran while one was open for 0% of the time, Pallas kernels for 13%

commit v1 on v0

v1 whole, which is shorter than its diff:
```python
import functools

import jax
import jax.numpy as jnp
from jax import lax
from jax.experimental import pallas as pl
from jax.experimental.pallas import tpu as pltpu
from jax.sharding import PartitionSpec as P

EPS = 1e-06


def normalize(rows):
    return rows * lax.rsqrt(jnp.mean(rows * rows, axis=-1, keepdims=True) + EPS)


def body_plain(tokens, gate_weight, up_weight, down_weight, in_gain, out_gain):
    groups = lax.axis_size("fs")
    rows_all = tokens.shape[0]
    rows_mine = rows_all // groups
    model_width = tokens.shape[1]
    local_rows = gate_weight.shape[1]
    block_width = gate_weight.shape[2] // groups
    residual = lax.dynamic_slice_in_dim(
        tokens, lax.axis_index("fs") * rows_mine, rows_mine, 0
    ).astype(jnp.float32)
    normed = normalize(tokens.astype(jnp.float32)).astype(jnp.bfloat16)
    gates = []
    ups = []
    downs = []
    rounded_state = tokens
    contract_last = (((1,), (1,)), ((), ()))
    for section_idx in range(2):
        scale = in_gain[section_idx][:, None]
        gate_rounded = (scale * gate_weight[section_idx]).astype(jnp.bfloat16)
        up_rounded = (scale * up_weight[section_idx]).astype(jnp.bfloat16)
        down_rounded = down_weight[section_idx].astype(jnp.bfloat16)
        flipped = [
            w.T.reshape(groups, block_width, local_rows)
            for w in (gate_rounded, up_rounded, down_rounded)
        ]
        arrived = (
            lax.all_to_all(flipped[0], "fs", split_axis=0, concat_axis=2, tiled=True),
            lax.all_to_all(flipped[1], "fs", split_axis=0, concat_axis=2, tiled=True),
            lax.all_to_all(flipped[2], "fs", split_axis=0, concat_axis=2, tiled=True),
        )
        thin_rows = [w.reshape(block_width, model_width) for w in arrived]
        sampler_mats = (
            lax.all_gather(thin_rows[0], "tp", axis=0, tiled=True),
            lax.all_gather(thin_rows[1], "tp", axis=0, tiled=True),
            lax.all_gather(thin_rows[2], "tp", axis=0, tiled=True),
        )
        gate_flip, up_flip, down_flip = (sampler_mats[0], sampler_mats[1], sampler_mats[2])
        gates.append(gate_flip.T)
        ups.append(up_flip.T)
        downs.append(down_flip.T)

        def hidden_of(row_block):
            gate_act = lax.dot_general(
                row_block, gate_flip, contract_last, preferred_element_type=jnp.float32
            )
            up_act = lax.dot_general(
                row_block, up_flip, contract_last, preferred_element_type=jnp.float32
            )
            return (jax.nn.silu(gate_act) * up_act).astype(jnp.bfloat16)

        if section_idx == 0:
            hidden = hidden_of(normed)
        else:
            hidden = hidden_of(lax.all_gather(normed, "fs", axis=0, tiled=True))
        mixed = lax.psum_scatter(
            jnp.dot(hidden, down_flip, preferred_element_type=jnp.float32),
            "fs",
            scatter_dimension=0,
            tiled=True,
        )
        rounded_state = (residual + 0.5 * out_gain[section_idx] * normalize(mixed)).astype(
            jnp.bfloat16
        )
        if section_idx == 0:
            residual = rounded_state.astype(jnp.float32)
            normed = normalize(residual).astype(jnp.bfloat16)
    return (jnp.stack(gates), jnp.stack(ups), jnp.stack(downs), rounded_state)


ORDER = (0, 3, 1, 2)
TURNED = ((0, 3), (2, 3), (4, 3))
LAST = (((1,), (1,)), ((), ()))
MESH = pl.DeviceIdType.MESH


def cuts(extent, width):
    return [(start, min(width, extent - start)) for start in range(0, extent, width)]


def fused_kernel(tokens, gate_w, up_w, down_w, in_gain, out_gain, *refs):
    full, state = refs[:6], refs[6]
    stage, flip, tok, normed, hidden, part, rin, lin, rout, lout, rs_r, rs_l = refs[7:19]
    load_sem, tok_sem, send_sem, recv_sem = refs[19:]
    y, z, t = lax.axis_index("grp"), lax.axis_index("fs"), lax.axis_index("tp")
    x, c = t // 2, lax.rem(t, 2)
    other_y, other_x, other_c = 1 - y, (1 - x) * 2 + c, x * 2 + (1 - c)
    other_both = (1 - x) * 2 + (1 - c)
    groups = 4
    ahead, behind = lax.rem(z + 1, groups), lax.rem(z + groups - 1, groups)
    to_x, to_c, to_y = {"tp": other_x}, {"tp": other_c}, {"grp": other_y}
    to_right, to_left = {"fs": ahead}, {"fs": behind}
    inner = (z > 0) & (z < groups - 1)
    _, rows, cols = gate_w.shape
    half_rows = rows // 2
    block = cols // groups
    half = block // 2
    count, width = tokens.shape
    quarter = count // groups
    piece = count // 8
    f32, bf16 = jnp.float32, jnp.bfloat16
    weights = (gate_w, up_w, down_w)

    names = []
    sent = []

    def slot(name):
        if name not in names:
            names.append(name)
        return names.index(name)

    def remote(name, source, target, device):
        k = slot(name)
        return pltpu.make_async_remote_copy(
            src_ref=source,
            dst_ref=target,
            send_sem=send_sem.at[k],
            recv_sem=recv_sem.at[k],
            device_id=device,
            device_id_type=MESH,
        )

    def send(name, source, target, device):
        copy = remote(name, source, target, device)
        copy.start()
        return copy

    def arrived(name, landed, device):
        remote(name, landed, landed, device).wait_recv()

    def slabs(start, extent, step, work):
        def one(i, carry):
            work(pl.ds(pl.multiple_of(start + i * step, step), step))
            return carry

        lax.fori_loop(0, extent // step, one, 0)

    def place(m, column, which, source):
        top = pl.multiple_of(column * block + which * half, 16)
        return full[m].at[pl.ds(top, half), pl.ds(pl.multiple_of(source * rows, 128), rows)]

    def blocks_of(m, column, source):
        top = pl.multiple_of(column * block, 16)
        return full[m].at[pl.ds(top, block), pl.ds(pl.multiple_of(source * rows, 128), rows)]

    def rows_of(m, column):
        return full[m].at[pl.ds(pl.multiple_of(column * block, 16), block), :]

    def origin(shift):
        return lax.rem(z + groups - shift, groups)

    def load(k):
        m, r = k // 2, k % 2
        return pltpu.make_async_copy(
            weights[m % 3].at[m // 3, pl.ds(r * half_rows, half_rows), :],
            stage.at[k % 2],
            load_sem.at[k % 2],
        )

    fetch = []
    for p, chunk in enumerate(ORDER):
        fetch.append(
            pltpu.make_async_copy(
                tokens.at[pl.ds(chunk * quarter, quarter), :],
                tok.at[pl.ds(p * quarter, quarter), :],
                tok_sem.at[p],
            )
        )
    load(0).start()
    load(1).start()
    for copy in fetch:
        copy.start()

    partners = [{"fs": lax.rem(z + shift, groups)} for shift in range(1, groups)]
    partners += [to_x, to_c, to_y]
    barrier = pltpu.get_barrier_semaphore()
    for partner in partners:
        pl.semaphore_signal(barrier, inc=1, device_id=partner, device_id_type=MESH)

    z_sends = {}

    def prep(m):
        layer, which, s = m // 3, m % 3, m % 3
        if m >= 3:
            for copy in z_sends[m - 3]:
                copy.wait_send()
        for r in range(2):
            k = 2 * m + r
            load(k).wait()
            lanes = slice(r * half_rows, (r + 1) * half_rows)

            def one(i, carry):
                cut = pl.ds(pl.multiple_of(i * 128, 128), 128)
                turned = stage[k % 2, :, cut].T
                if which < 2:
                    turned = turned * in_gain[layer : layer + 1, lanes]
                flip[s, cut, lanes] = turned.astype(bf16)
                return carry

            lax.fori_loop(0, cols // 128, one, 0)
            if k + 2 < 12:
                load(k + 2).start()
        mine = flip[s, pl.ds(pl.multiple_of(z * block, 16), block), :]
        top = pl.multiple_of(t * block, 16)
        full[m][pl.ds(top, block), pl.ds(pl.multiple_of(z * rows, 128), rows)] = mine

    def send_z(m):
        z_sends[m] = []
        for shift in range(1, groups):
            target = lax.rem(z + shift, groups)
            top = pl.multiple_of(target * block + y * half, 16)
            source = flip.at[m % 3, pl.ds(top, half), :]
            z_sends[m].append(send(("z", m, shift), source, place(m, t, y, z), {"fs": target}))

    def send_x(m):
        spot = blocks_of(m, t, z)
        sent.append(send(("x", m, 0), spot, spot, to_x))

    def on_z(m, shift):
        source = origin(shift)
        spot = place(m, t, y, source)
        arrived(("z", m, shift), spot, {"fs": source})
        sent.append(send(("x", m, shift), spot, spot, to_x))
        sent.append(send(("y", m, shift), spot, spot, to_y))

    def on_x(m, shift):
        source = origin(shift)
        spot = place(m, other_x, y, source)
        arrived(("x", m, shift), spot, to_x)
        if (m, shift) not in TURNED:
            sent.append(send(("w", m, shift), spot, spot, to_y))

    def finish(m):
        arrived(("x", m, 0), blocks_of(m, other_x, z), to_x)
        for shift in range(1, groups):
            spot = place(m, t, other_y, origin(shift))
            arrived(("y", m, shift), spot, to_y)
            if (m, shift) in TURNED:
                sent.append(send(("w", m, shift), spot, spot, to_x))
        mine = rows_of(m, t)
        sent.append(send(("c", m, 0), mine, mine, to_c))
        for shift in range(1, groups):
            device = to_x if (m, shift) in TURNED else to_y
            arrived(("w", m, shift), place(m, other_x, other_y, origin(shift)), device)
        mine = rows_of(m, other_x)
        sent.append(send(("c", m, 1), mine, mine, to_c))

    def on_c(m):
        arrived(("c", m, 0), rows_of(m, other_c), to_c)
        arrived(("c", m, 1), rows_of(m, other_both), to_c)

    def scaled(value):
        return value * lax.rsqrt(jnp.mean(value * value, axis=-1, keepdims=True) + EPS)

    def gated(layer, start, extent, cut):
        first, size = cut
        line = normed[start : start + extent, :]
        gate = lax.dot_general(
            line, full[3 * layer][first : first + size, :], LAST, preferred_element_type=f32
        )
        lift = lax.dot_general(
            line, full[3 * layer + 1][first : first + size, :], LAST, preferred_element_type=f32
        )
        value = jax.nn.silu(gate) * lift
        hidden[start : start + extent, first : first + size] = value.astype(bf16)

    def summed(layer, start, extent):
        line = hidden[start : start + extent, :]
        for first, size in cuts(width, 512):
            part[start : start + extent, first : first + size] = jnp.dot(
                line, full[3 * layer + 2][:, first : first + size], preferred_element_type=f32
            ).astype(bf16)

    def add_into(target, landed, offset, start, extent):
        def work(line):
            other = landed[line, :] if offset is None else landed[offset, line, :]
            total = other.astype(f32) + part[line, :].astype(f32)
            target[line, :] = total.astype(bf16)

        slabs(start, extent, 32, work)

    def lines(j):
        return pl.ds(j * piece, piece)

    def pass_right(j):
        arrived(("R", j), rin.at[lines(j), :], to_left)
        add_into(rout, rin, None, j * piece, piece)
        send(("R", j), rout.at[lines(j), :], rin.at[lines(j), :], to_right)

    def pass_left(j):
        arrived(("L", j), lin.at[lines(j), :], to_right)
        add_into(lout, lin, None, j * piece, piece)
        send(("L", j), lout.at[lines(j), :], lin.at[lines(j), :], to_left)

    def near(j):
        @pl.when(z == 1)
        def _():
            pass_right(j)

        @pl.when(z == 2)
        def _():
            pass_left(j)

    def edge(j):
        @pl.when(z == 0)
        def _():
            send(("R", j), part.at[lines(j), :], rin.at[lines(j), :], to_right)

        @pl.when(z == groups - 1)
        def _():
            send(("L", j), part.at[lines(j), :], lin.at[lines(j), :], to_left)

    def far(j):
        @pl.when(z == 1)
        def _():
            pass_left(j)

        @pl.when(z == 2)
        def _():
            pass_right(j)

    def settle(j):
        @pl.when(z == 0)
        def _():
            arrived(("L", j), lin.at[lines(j), :], to_right)

        @pl.when(z == groups - 1)
        def _():
            arrived(("R", j), rin.at[lines(j), :], to_left)

        def work(line):
            total = part[line, :].astype(f32) + rin[line, :].astype(f32) + lin[line, :].astype(f32)
            after = tok[line, :].astype(f32) + 0.5 * out_gain[0:1, :] * scaled(total)
            after = after.astype(bf16)
            tok[line, :] = after
            normed[line, :] = scaled(after.astype(f32)).astype(bf16)

        slabs(j * piece, piece, 32, work)

    def exchange(i):
        if i < 8:
            near(i)
        if 0 <= i - 1 < 8:
            far(i - 1)
        if 0 <= i - 2 < 8:
            settle(i - 2)

    def exchange_sent():
        for j in range(8):

            @pl.when(z < groups - 1)
            def _():
                remote(("R", j), rout.at[lines(j), :], rin.at[lines(j), :], to_right).wait_send()

            @pl.when(z > 0)
            def _():
                remote(("L", j), lout.at[lines(j), :], lin.at[lines(j), :], to_left).wait_send()

    def block_at(k):
        return pl.ds(ORDER.index(k) * quarter, quarter)

    def reduce_right(k):
        start = ORDER.index(k) * quarter

        @pl.when(z == 0)
        def _():
            send(("r", k), part.at[block_at(k), :], rs_r.at[block_at(k), :], to_right)

        @pl.when((z > 0) & (z < k))
        def _():
            arrived(("r", k), rs_r.at[block_at(k), :], to_left)
            add_into(rout, rs_r, None, start, quarter)
            send(("r", k), rout.at[block_at(k), :], rs_r.at[block_at(k), :], to_right)

    def reduce_left(k):
        start = ORDER.index(k) * quarter

        @pl.when(z == groups - 1)
        def _():
            send(("l", k), part.at[block_at(k), :], rs_l.at[block_at(k), :], to_left)

        @pl.when((z < groups - 1) & (z > k))
        def _():
            arrived(("l", k), rs_l.at[block_at(k), :], to_right)
            add_into(lout, rs_l, None, start, quarter)
            send(("l", k), lout.at[block_at(k), :], rs_l.at[block_at(k), :], to_left)

    def conclude():
        for k in range(groups):

            @pl.when(z == k)
            def _():
                if k > 0:
                    arrived(("r", k), rs_r.at[block_at(k), :], to_left)
                if k < groups - 1:
                    arrived(("l", k), rs_l.at[block_at(k), :], to_right)
                start = ORDER.index(k) * quarter

                def work(line):
                    total = part[line, :].astype(f32)
                    if k > 0:
                        total += rs_r[line, :].astype(f32)
                    if k < groups - 1:
                        total += rs_l[line, :].astype(f32)
                    after = tok[line, :].astype(f32) + 0.5 * out_gain[1:2, :] * scaled(total)
                    state[pl.ds(line.start - start, 32), :] = after.astype(bf16)

                slabs(start, quarter, 32, work)

        for k in range(1, groups):

            @pl.when(z < k)
            def _():
                remote(("r", k), rout.at[block_at(k), :], rout.at[block_at(k), :], to_right).wait_send()

        for k in range(groups - 1):

            @pl.when(z > k)
            def _():
                remote(("l", k), lout.at[block_at(k), :], lout.at[block_at(k), :], to_left).wait_send()

    prep(0)
    pl.semaphore_wait(barrier, len(partners))
    send_z(0)
    send_x(0)
    for m in (1, 2):
        prep(m)
        send_z(m)
        send_x(m)
    for copy in fetch:
        copy.wait()

    def first_norm(line):
        normed[line, :] = scaled(tok[line, :].astype(f32)).astype(bf16)

    slabs(0, count, 32, first_norm)

    @pl.when(z == 0)
    def _():
        rin[...] = jnp.zeros_like(rin)

    @pl.when(z == groups - 1)
    def _():
        lin[...] = jnp.zeros_like(lin)

    pieces = cuts(cols, 384)
    whole = (0, count)
    upper, lower = (0, count // 2), (count // 2, count // 2)

    on_z(0, 1)
    on_z(0, 2)
    on_x(0, 1)
    on_z(0, 3)
    on_x(0, 2)
    on_z(1, 1)
    on_x(0, 3)
    prep(3)
    send_z(3)
    send_x(3)
    on_z(1, 2)
    on_x(1, 1)
    on_z(1, 3)
    on_x(1, 2)
    finish(0)
    on_z(2, 1)
    on_x(1, 3)
    on_z(2, 2)
    on_x(2, 1)
    on_z(2, 3)
    prep(4)
    send_z(4)
    send_x(4)
    finish(1)
    on_x(2, 2)
    on_z(3, 1)
    on_c(0)
    on_c(1)
    gated(0, *whole, pieces[0])
    on_x(2, 3)
    on_z(3, 2)
    gated(0, *whole, pieces[1])
    on_z(3, 3)
    on_x(3, 1)
    gated(0, *whole, pieces[2])
    gated(0, *whole, pieces[3])
    finish(2)
    on_x(3, 2)
    on_c(2)
    summed(0, *upper)
    for j in range(4):
        edge(j)
    summed(0, *lower)
    for j in range(4, 8):
        edge(j)
    on_z(4, 1)
    on_x(3, 3)
    on_z(4, 2)
    on_x(4, 1)
    on_z(4, 3)
    prep(5)
    exchange(0)
    finish(3)
    exchange(1)
    on_x(4, 2)
    exchange(2)
    send_z(5)
    send_x(5)
    on_x(4, 3)
    exchange(3)
    exchange(4)
    on_z(5, 1)
    exchange(5)
    on_z(5, 2)
    on_x(5, 1)
    finish(4)
    exchange(6)
    on_z(5, 3)
    on_x(5, 2)
    on_c(3)
    on_c(4)
    exchange(7)
    for cut in pieces:
        gated(1, *upper, cut)
    on_x(5, 3)
    exchange(8)
    exchange(9)
    for cut in pieces:
        gated(1, *lower, cut)
    exchange_sent()
    finish(5)
    on_c(5)
    summed(1, *upper)
    reduce_right(3)
    reduce_left(0)
    summed(1, *lower)
    reduce_right(2)
    reduce_left(1)
    reduce_right(1)
    reduce_left(2)
    conclude()
    for m in (3, 4, 5):
        sent.extend(z_sends[m])
    for copy in sent:
        copy.wait_send()


def fused(tokens, gate_weight, up_weight, down_weight, in_gain, out_gain):
    count, width = tokens.shape
    _, rows, cols = gate_weight.shape
    bf16 = jnp.bfloat16
    quarter = count // 4
    whole = pl.BlockSpec(memory_space=pl.ANY)
    near = pl.BlockSpec(memory_space=pltpu.VMEM)
    band = pltpu.VMEM((count, width), bf16)
    messages = 128
    return pl.pallas_call(
        fused_kernel,
        in_specs=[whole] * 4 + [near] * 2,
        out_specs=[near] * 7,
        out_shape=[pltpu.VMEM((cols, width), bf16)] * 6 + [pltpu.VMEM((quarter, width), bf16)],
        scratch_shapes=[
            pltpu.VMEM((2, rows // 2, cols), jnp.float32),
            pltpu.VMEM((3, cols, rows), bf16),
            band,
            band,
            pltpu.VMEM((count, cols), bf16),
            band,
            band,
            band,
            band,
            band,
            band,
            band,
            pltpu.SemaphoreType.DMA((2,)),
            pltpu.SemaphoreType.DMA((4,)),
            pltpu.SemaphoreType.DMA((messages,)),
            pltpu.SemaphoreType.DMA((messages,)),
        ],
        compiler_params=pltpu.CompilerParams(
            collective_id=0, has_side_effects=True, vmem_limit_bytes=29 * 2**20
        ),
    )(tokens, gate_weight, up_weight, down_weight, in_gain, out_gain)


def emit_kernel(*refs):
    flips, state = refs[:6], refs[6]
    outs, result = refs[7:10], refs[10]
    held, sems, state_sem = refs[11:]
    slots, step, _ = held.shape
    width = flips[0].shape[1]
    steps = width // step
    last = pltpu.make_async_copy(state, result, state_sem)
    last.start()

    def out_copy(k, i):
        slot = lax.rem(i, slots)
        top = pl.multiple_of(i * step, step)
        return pltpu.make_async_copy(
            held.at[slot], outs[k % 3].at[k // 3, pl.ds(top, step), :], sems.at[slot]
        )

    for k in range(6):

        def one(i, carry):
            if k == 0:

                @pl.when(i >= slots)
                def _():
                    out_copy(k, i).wait()

            else:
                out_copy(k, i).wait()
            held[lax.rem(i, slots)] = flips[k][:, pl.ds(pl.multiple_of(i * step, step), step)].T
            out_copy(k, i).start()
            return carry

        lax.fori_loop(0, steps, one, 0)
    for i in range(slots):
        out_copy(5, steps - slots + i).wait()
    last.wait()


def emit(flips, state):
    cols, width = flips[0].shape
    near = pl.BlockSpec(memory_space=pltpu.VMEM)
    whole = pl.BlockSpec(memory_space=pl.ANY)
    return pl.pallas_call(
        emit_kernel,
        in_specs=[near] * 7,
        out_specs=[whole] * 4,
        out_shape=[jax.ShapeDtypeStruct((2, width, cols), jnp.bfloat16)] * 3
        + [jax.ShapeDtypeStruct(state.shape, jnp.bfloat16)],
        scratch_shapes=[
            pltpu.VMEM((8, 256, cols), jnp.bfloat16),
            pltpu.SemaphoreType.DMA((8,)),
            pltpu.SemaphoreType.DMA,
        ],
        compiler_params=pltpu.CompilerParams(vmem_limit_bytes=16 * 2**20),
    )(*flips, state)


def body(tokens, gate_weight, up_weight, down_weight, in_gain, out_gain):
    groups, halves = lax.axis_size("fs"), lax.axis_size("grp")
    columns = lax.axis_size("tp")
    count, model_width = tokens.shape
    _, rows, cols = gate_weight.shape
    odd = cols % (32 * groups) or rows % 256 or cols % 128 or count % 512 or model_width % 2048
    if odd or halves != 2 or columns != 4 or groups != 4:
        return body_plain(tokens, gate_weight, up_weight, down_weight, in_gain, out_gain)
    *flips, state = fused(tokens, gate_weight, up_weight, down_weight, in_gain, out_gain)
    return tuple(emit(flips, state))


def solution(mesh):
    in_specs = (
        P(("grp", "tp"), None),
        P(None, "fs", "tp"),
        P(None, "fs", "tp"),
        P(None, "fs", "tp"),
        P(None, "fs"),
        P(),
    )
    out_specs = (
        P("grp", None, "fs"),
        P("grp", None, "fs"),
        P("grp", None, "fs"),
        P(("grp", "tp", "fs"), None),
    )
    return jax.shard_map(body, mesh=mesh, in_specs=in_specs, out_specs=out_specs, check_vma=False)
```

time: 385 us -> 289 us (0.75)
  waiting for transfers between devices: 84.5 us -> 0 us
  matrix products: 42.8 us -> 0 us
  Pallas kernels: 233 us -> 267 us
  local copies, waits for them, and re-layouts: 1.72 us -> 20.6 us
  between operations: 13.8 us -> 0.82 us
  other arithmetic: 7.5 us -> 0 us
    reduce_scatter x2 -> x0, waiting for transfers between devices: 47.8 us -> none  [body(): mixed = lax.psum_scatter(partial, 'fs', scatter_dimension=0, tiled=True)]
    dot_general x4 -> x0, matrix products: 42.8 us -> none  [the longest x2 26.7 us: body(): jnp.dot(hidden, down_flip, preferred_element_type=jnp.float32)]
    all_gather x1 -> x0, waiting for transfers between devices: 36.6 us -> none  [body(): normed = lax.all_gather(normed, 'fs', axis=0, tiled=True)]
    pallas_call x13 -> x2, Pallas kernels: 233 us -> 267 us  [the longest x1 254 us: fused(): pl.pallas_call(fused_kernel, in_specs=[whole] * 4 + [near] * 2, out_specs...]
    unnamed x6 -> x16, local copies, waits for them, and re-layouts: 0.01 us -> 20.6 us
    reduce_sum x4 -> x0, other arithmetic: 4.39 us -> none  [normalize(): return rows * lax.rsqrt(jnp.mean(rows * rows, axis=-1, keepdims=True) + EPS)]
  transfers between devices with their start and end apart: 3 -> 0, of which waited for: 3 -> 0; matrix products, arithmetic and copies ran while one was open for 0% -> 0% of each run, Pallas kernels for 13% -> 0%
where the time goes in v1:
time: 289 us; the launch traced here: 288 us
  Pallas kernels  267 us (92%)
  local copies, waits for them, and re-layouts  20.6 us (7%)
    pallas_call x1, Pallas kernels, fused(): pl.pallas_call(fused_kernel, in_specs=[whole] * 4 + [near] * 2, out_specs...  254 us
    unnamed x16, local copies, waits for them, and re-layouts  20.6 us
    pallas_call x1, Pallas kernels, emit(): pl.pallas_call(emit_kernel, in_specs=[near] * 7, out_specs=[whole] * 4, o...  12.9 us

profile of v1, /device:TPU:0, one launch (start us, length us, event | category | flops | bytes accessed | tf_op | source)
XLA Modules:
  0.0 288.4 jit_solution(14500813481649057720)
XLA Ops:
  0.6 254.1 %shard_map.93 = (bf16[1408,2048]{1,0:T(8,128)(2,1)S(1)}, bf16[1408,2048]{1,0:T(8,128)(2,1)S(1)}, bf16[1408,2048]{1,0:T(8,128)(2,1)S(1)}, bf16[1408,2048]{1,0:T(8...) custom-call(bf16[512,2048]{1,0:T(8,128)(2,1)} %tokens.1, ...), custom_call_target="tpu_custom_call" | custom-call | tf_op jit(solution)/shard_map/pallas_call | solution.py:571
  254.8 0.0 copy-start
  254.8 2.5 copy-done
  257.3 0.0 copy-start.2
  257.3 2.5 copy-done.2
  259.8 0.0 copy-start.4
  259.8 2.5 copy-done.4
  262.4 0.0 copy-start.6
  262.4 2.5 copy-done.6
  264.8 0.0 copy-start.1
  264.8 2.6 copy-done.1
  267.5 0.0 copy-start.3
  267.5 2.6 copy-done.3
  270.1 0.0 copy-start.5
  270.1 2.6 copy-done.5
  272.8 0.0 copy-start.7
  272.8 2.6 copy-done.7
  275.4 12.9 %shard_map.94 = (bf16[2,2048,1408]{2,1,0:T(8,128)(2,1)}, bf16[2,2048,1408]{2,1,0:T(8,128)(2,1)}, bf16[2,2048,1408]{2,1,0:T(8,128)(2,1)}, bf16[128,2048]{1,0:T(8,128)(2,1)}) custom-call(bf16[1408,2048]{1,0:T(8,128)(2,1)S(1)} %copy-done.1, bf16[1408,2048]{1,0:T(8,128)(2,1)S(1)} %copy-done.3, bf16[1408,2048]{1,0:T(8,128)(2,1)S(1)} %copy-done.5, ...), custom_call_target="tpu_custom_call" | custom-call | tf_op jit(solution)/shard_map/pallas_call | solution.py:642
Async XLA Ops:
  254.8 2.5 copy-start
  257.3 2.5 copy-start.2
  259.8 2.5 copy-start.4
  262.4 2.5 copy-start.6
  264.8 2.6 copy-start.1
  267.5 2.6 copy-start.3
  270.1 2.6 copy-start.5
  272.8 2.6 copy-start.7

commit v2 on v1

--- a/solution.py
+++ b/solution.py
@@ -84,7 +84,7 @@
 
 
 ORDER = (0, 3, 1, 2)
-TURNED = ((0, 3), (2, 3), (4, 3))
+TURNED = ((0, 1), (2, 1), (4, 1))
 LAST = (((1,), (1,)), ((), ()))
 MESH = pl.DeviceIdType.MESH
 
@@ -94,9 +94,11 @@
 
 
 def fused_kernel(tokens, gate_w, up_w, down_w, in_gain, out_gain, *refs):
-    full, state = refs[:6], refs[6]
-    stage, flip, tok, normed, hidden, part, rin, lin, rout, lout, rs_r, rs_l = refs[7:19]
-    load_sem, tok_sem, send_sem, recv_sem = refs[19:]
+    cols = gate_w.shape[2]
+    full = [refs[0].at[pl.ds(m * cols, cols), :] for m in range(6)]
+    state = refs[0]
+    stage, flip, tok, normed, hidden, part, rin, lin, rout, lout, rs_r, rs_l = refs[1:13]
+    load_sem, tok_sem, send_sem, recv_sem = refs[13:]
     y, z, t = lax.axis_index("grp"), lax.axis_index("fs"), lax.axis_index("tp")
     x, c = t // 2, lax.rem(t, 2)
     other_y, other_x, other_c = 1 - y, (1 - x) * 2 + c, x * 2 + (1 - c)
@@ -161,8 +163,8 @@
     def rows_of(m, column):
         return full[m].at[pl.ds(pl.multiple_of(column * block, 16), block), :]
 
-    def origin(shift):
-        return lax.rem(z + groups - shift, groups)
+    def origin(order):
+        return (z + 1 - 2 * lax.rem(z, 2), 2 - z // 2, 3 * (1 - z // 2))[order - 1]
 
     def load(k):
         m, r = k // 2, k % 2
@@ -221,11 +223,22 @@
 
     def send_z(m):
         z_sends[m] = []
-        for shift in range(1, groups):
-            target = lax.rem(z + shift, groups)
+        base = [slot(("z", m, order)) for order in range(1, groups)][0]
+        outer = 1 - (lax.rem(z, 3) + 1) // 2
+        for order in range(1, groups):
+            target = origin(order)
             top = pl.multiple_of(target * block + y * half, 16)
-            source = flip.at[m % 3, pl.ds(top, half), :]
-            z_sends[m].append(send(("z", m, shift), source, place(m, t, y, z), {"fs": target}))
+            landing = base if order == 1 else base + 1 + outer
+            copy = pltpu.make_async_remote_copy(
+                src_ref=flip.at[m % 3, pl.ds(top, half), :],
+                dst_ref=place(m, t, y, z),
+                send_sem=send_sem.at[base + order - 1],
+                recv_sem=recv_sem.at[landing],
+                device_id={"fs": target},
+                device_id_type=MESH,
+            )
+            copy.start()
+            z_sends[m].append(copy)
 
     def send_x(m):
         spot = blocks_of(m, t, z)
@@ -239,19 +252,22 @@
         sent.append(send(("y", m, shift), spot, spot, to_y))
 
     def on_x(m, shift):
-        source = origin(shift)
-        spot = place(m, other_x, y, source)
+        spot = place(m, other_x, y, origin(shift))
         arrived(("x", m, shift), spot, to_x)
-        if (m, shift) not in TURNED:
-            sent.append(send(("w", m, shift), spot, spot, to_y))
+        sent.append(send(("w", m, shift), spot, spot, to_y))
+
+    def turn(m, order):
+        spot = place(m, t, other_y, origin(order))
+        arrived(("y", m, order), spot, to_y)
+        sent.append(send(("w", m, order), spot, spot, to_x))
 
     def finish(m):
         arrived(("x", m, 0), blocks_of(m, other_x, z), to_x)
         for shift in range(1, groups):
-            spot = place(m, t, other_y, origin(shift))
-            arrived(("y", m, shift), spot, to_y)
             if (m, shift) in TURNED:
-                sent.append(send(("w", m, shift), spot, spot, to_x))
+                arrived(("x", m, shift), place(m, other_x, y, origin(shift)), to_x)
+            else:
+                arrived(("y", m, shift), place(m, t, other_y, origin(shift)), to_y)
         mine = rows_of(m, t)
         sent.append(send(("c", m, 0), mine, mine, to_c))
         for shift in range(1, groups):
@@ -360,8 +376,8 @@
         if 0 <= i - 2 < 8:
             settle(i - 2)
 
-    def exchange_sent():
-        for j in range(8):
+    def exchange_sent(first, last):
+        for j in range(first, last):
 
             @pl.when(z < groups - 1)
             def _():
@@ -371,83 +387,98 @@
             def _():
                 remote(("L", j), lout.at[lines(j), :], lin.at[lines(j), :], to_left).wait_send()
 
-    def block_at(k):
-        return pl.ds(ORDER.index(k) * quarter, quarter)
-
-    def reduce_right(k):
-        start = ORDER.index(k) * quarter
-
+    def parts_of(k):
+        return [j for j in range(8) if ORDER[j // 2] == k]
+
+    def reduce_edge(rightward, leftward):
         @pl.when(z == 0)
         def _():
-            send(("r", k), part.at[block_at(k), :], rs_r.at[block_at(k), :], to_right)
-
-        @pl.when((z > 0) & (z < k))
-        def _():
-            arrived(("r", k), rs_r.at[block_at(k), :], to_left)
-            add_into(rout, rs_r, None, start, quarter)
-            send(("r", k), rout.at[block_at(k), :], rs_r.at[block_at(k), :], to_right)
-
-    def reduce_left(k):
-        start = ORDER.index(k) * quarter
+            for j in parts_of(rightward):
+                send(("r", j), part.at[lines(j), :], rs_r.at[lines(j), :], to_right)
 
         @pl.when(z == groups - 1)
         def _():
-            send(("l", k), part.at[block_at(k), :], rs_l.at[block_at(k), :], to_left)
-
-        @pl.when((z < groups - 1) & (z > k))
-        def _():
-            arrived(("l", k), rs_l.at[block_at(k), :], to_right)
-            add_into(lout, rs_l, None, start, quarter)
-            send(("l", k), lout.at[block_at(k), :], rs_l.at[block_at(k), :], to_left)
+            for j in parts_of(leftward):
+                send(("l", j), part.at[lines(j), :], rs_l.at[lines(j), :], to_left)
+
+    def reduce_right(j):
+        arrived(("r", j), rs_r.at[lines(j), :], to_left)
+        add_into(rout, rs_r, None, j * piece, piece)
+        send(("r", j), rout.at[lines(j), :], rs_r.at[lines(j), :], to_right)
+
+    def reduce_left(j):
+        arrived(("l", j), rs_l.at[lines(j), :], to_right)
+        add_into(lout, rs_l, None, j * piece, piece)
+        send(("l", j), lout.at[lines(j), :], rs_l.at[lines(j), :], to_left)
+
+    def reduce_all():
+        zeros, ones, twos, threes = [parts_of(k) for k in range(groups)]
+
+        @pl.when(z == 1)
+        def _():
+            reduce_right(threes[0])
+            reduce_right(threes[1])
+            reduce_left(zeros[0])
+            reduce_right(twos[0])
+            reduce_left(zeros[1])
+            reduce_right(twos[1])
+
+        @pl.when(z == 2)
+        def _():
+            reduce_left(zeros[0])
+            reduce_left(zeros[1])
+            reduce_right(threes[0])
+            reduce_left(ones[0])
+            reduce_right(threes[1])
+            reduce_left(ones[1])
 
     def conclude():
         for k in range(groups):
-
-            @pl.when(z == k)
-            def _():
-                if k > 0:
-                    arrived(("r", k), rs_r.at[block_at(k), :], to_left)
-                if k < groups - 1:
-                    arrived(("l", k), rs_l.at[block_at(k), :], to_right)
-                start = ORDER.index(k) * quarter
-
-                def work(line):
-                    total = part[line, :].astype(f32)
+            for j in parts_of(k):
+
+                @pl.when(z == k)
+                def _():
                     if k > 0:
-                        total += rs_r[line, :].astype(f32)
+                        arrived(("r", j), rs_r.at[lines(j), :], to_left)
                     if k < groups - 1:
-                        total += rs_l[line, :].astype(f32)
-                    after = tok[line, :].astype(f32) + 0.5 * out_gain[1:2, :] * scaled(total)
-                    state[pl.ds(line.start - start, 32), :] = after.astype(bf16)
-
-                slabs(start, quarter, 32, work)
-
-        for k in range(1, groups):
-
-            @pl.when(z < k)
-            def _():
-                remote(("r", k), rout.at[block_at(k), :], rout.at[block_at(k), :], to_right).wait_send()
-
-        for k in range(groups - 1):
-
-            @pl.when(z > k)
-            def _():
-                remote(("l", k), lout.at[block_at(k), :], lout.at[block_at(k), :], to_left).wait_send()
+                        arrived(("l", j), rs_l.at[lines(j), :], to_right)
+                    shift = 6 * cols - ORDER.index(k) * quarter
+
+                    def work(line):
+                        total = part[line, :].astype(f32)
+                        if k > 0:
+                            total += rs_r[line, :].astype(f32)
+                        if k < groups - 1:
+                            total += rs_l[line, :].astype(f32)
+                        after = tok[line, :].astype(f32) + 0.5 * out_gain[1:2, :] * scaled(total)
+                        state[pl.ds(line.start + shift, 32), :] = after.astype(bf16)
+
+                    slabs(j * piece, piece, 32, work)
+
+        for k in range(groups):
+            for j in parts_of(k):
+
+                @pl.when(z < k)
+                def _():
+                    remote(("r", j), rout.at[lines(j), :], rs_r.at[lines(j), :], to_right).wait_send()
+
+                @pl.when(z > k)
+                def _():
+                    remote(("l", j), lout.at[lines(j), :], rs_l.at[lines(j), :], to_left).wait_send()
 
     prep(0)
     pl.semaphore_wait(barrier, len(partners))
     send_z(0)
     send_x(0)
-    for m in (1, 2):
-        prep(m)
-        send_z(m)
-        send_x(m)
+    prep(1)
+    prep(2)
     for copy in fetch:
         copy.wait()
 
     def first_norm(line):
         normed[line, :] = scaled(tok[line, :].astype(f32)).astype(bf16)
 
+    on_z(0, 1)
     slabs(0, count, 32, first_norm)
 
     @pl.when(z == 0)
@@ -462,44 +493,48 @@
     whole = (0, count)
     upper, lower = (0, count // 2), (count // 2, count // 2)
 
-    on_z(0, 1)
     on_z(0, 2)
-    on_x(0, 1)
+    send_z(1)
+    turn(0, 1)
     on_z(0, 3)
     on_x(0, 2)
+    on_x(0, 3)
     on_z(1, 1)
-    on_x(0, 3)
-    prep(3)
-    send_z(3)
-    send_x(3)
     on_z(1, 2)
+    send_z(2)
+    finish(0)
     on_x(1, 1)
     on_z(1, 3)
+    send_x(1)
     on_x(1, 2)
-    finish(0)
+    on_x(1, 3)
     on_z(2, 1)
-    on_x(1, 3)
+    prep(3)
     on_z(2, 2)
-    on_x(2, 1)
+    send_z(3)
     on_z(2, 3)
     prep(4)
     send_z(4)
-    send_x(4)
+    on_x(2, 2)
     finish(1)
-    on_x(2, 2)
+    on_x(2, 3)
+    turn(2, 1)
+    send_x(2)
     on_z(3, 1)
+    prep(5)
     on_c(0)
     on_c(1)
     gated(0, *whole, pieces[0])
-    on_x(2, 3)
     on_z(3, 2)
+    send_z(5)
     gated(0, *whole, pieces[1])
     on_z(3, 3)
+    gated(0, *whole, pieces[2])
     on_x(3, 1)
-    gated(0, *whole, pieces[2])
     gated(0, *whole, pieces[3])
     finish(2)
     on_x(3, 2)
+    send_x(3)
     on_c(2)
     summed(0, *upper)
     for j in range(4):
@@ -507,51 +542,49 @@
     summed(0, *lower)
     for j in range(4, 8):
         edge(j)
+    on_x(3, 3)
     on_z(4, 1)
-    on_x(3, 3)
     on_z(4, 2)
-    on_x(4, 1)
     on_z(4, 3)
-    prep(5)
     exchange(0)
     finish(3)
     exchange(1)
+    turn(4, 1)
     on_x(4, 2)
     exchange(2)
-    send_z(5)
+    on_x(4, 3)
+    send_x(4)
+    on_z(5, 1)
+    on_z(5, 2)
+    exchange(3)
+    on_x(5, 1)
+    on_z(5, 3)
+    exchange(4)
+    finish(4)
     send_x(5)
-    on_x(4, 3)
-    exchange(3)
-    exchange(4)
-    on_z(5, 1)
     exchange(5)
-    on_z(5, 2)
-    on_x(5, 1)
-    finish(4)
+    on_x(5, 2)
     exchange(6)
-    on_z(5, 3)
-    on_x(5, 2)
+    on_x(5, 3)
     on_c(3)
     on_c(4)
-    exchange(7)
     for cut in pieces:
         gated(1, *upper, cut)
-    on_x(5, 3)
+    exchange(7)
+    finish(5)
     exchange(8)
+    on_c(5)
+    exchange_sent(0, 4)
+    summed(1, *upper)
+    reduce_edge(3, 0)
     exchange(9)
     for cut in pieces:
         gated(1, *lower, cut)
-    exchange_sent()
-    finish(5)
-    on_c(5)
-    summed(1, *upper)
-    reduce_right(3)
-    reduce_left(0)
+    exchange_sent(4, 8)
     summed(1, *lower)
-    reduce_right(2)
-    reduce_left(1)
-    reduce_right(1)
-    reduce_left(2)
+    reduce_edge(2, 1)
+    reduce_edge(1, 2)
+    reduce_all()
     conclude()
     for m in (3, 4, 5):
         sent.extend(z_sends[m])
@@ -571,8 +604,8 @@
     return pl.pallas_call(
         fused_kernel,
         in_specs=[whole] * 4 + [near] * 2,
-        out_specs=[near] * 7,
-        out_shape=[pltpu.VMEM((cols, width), bf16)] * 6 + [pltpu.VMEM((quarter, width), bf16)],
+        out_specs=near,
+        out_shape=pltpu.VMEM((6 * cols + quarter, width), bf16),
         scratch_shapes=[
             pltpu.VMEM((2, rows // 2, cols), jnp.float32),
             pltpu.VMEM((3, cols, rows), bf16),
@@ -597,14 +630,14 @@
     )(tokens, gate_weight, up_weight, down_weight, in_gain, out_gain)
 
 
-def emit_kernel(*refs):
-    flips, state = refs[:6], refs[6]
-    outs, result = refs[7:10], refs[10]
-    held, sems, state_sem = refs[11:]
-    slots, step, _ = held.shape
-    width = flips[0].shape[1]
+def emit_kernel(flips, *refs):
+    outs, result = refs[:3], refs[3]
+    held, sems, state_sem = refs[4:]
+    slots, step, cols = held.shape
+    width = flips.shape[1]
     steps = width // step
-    last = pltpu.make_async_copy(state, result, state_sem)
+    quarter = flips.shape[0] - 6 * cols
+    last = pltpu.make_async_copy(flips.at[pl.ds(6 * cols, quarter), :], result, state_sem)
     last.start()
 
     def out_copy(k, i):
@@ -625,7 +658,8 @@
 
             else:
                 out_copy(k, i).wait()
-            held[lax.rem(i, slots)] = flips[k][:, pl.ds(pl.multiple_of(i * step, step), step)].T
+            lanes = pl.ds(pl.multiple_of(i * step, step), step)
+            held[lax.rem(i, slots)] = flips[k * cols : (k + 1) * cols, lanes].T
             out_copy(k, i).start()
             return carry
 
@@ -635,23 +669,23 @@
     last.wait()
 
 
-def emit(flips, state):
-    cols, width = flips[0].shape
+def emit(flips, cols):
+    height, width = flips.shape
     near = pl.BlockSpec(memory_space=pltpu.VMEM)
     whole = pl.BlockSpec(memory_space=pl.ANY)
     return pl.pallas_call(
         emit_kernel,
-        in_specs=[near] * 7,
+        in_specs=[near],
         out_specs=[whole] * 4,
         out_shape=[jax.ShapeDtypeStruct((2, width, cols), jnp.bfloat16)] * 3
-        + [jax.ShapeDtypeStruct(state.shape, jnp.bfloat16)],
+        + [jax.ShapeDtypeStruct((height - 6 * cols, width), jnp.bfloat16)],
         scratch_shapes=[
             pltpu.VMEM((8, 256, cols), jnp.bfloat16),
             pltpu.SemaphoreType.DMA((8,)),
             pltpu.SemaphoreType.DMA,
         ],
-        compiler_params=pltpu.CompilerParams(vmem_limit_bytes=16 * 2**20),
-    )(*flips, state)
+        compiler_params=pltpu.CompilerParams(vmem_limit_bytes=8 * 2**20),
+    )(flips)
 
 
 def body(tokens, gate_weight, up_weight, down_weight, in_gain, out_gain):
@@ -662,8 +696,8 @@
     odd = cols % (32 * groups) or rows % 256 or cols % 128 or count % 512 or model_width % 2048
     if odd or halves != 2 or columns != 4 or groups != 4:
         return body_plain(tokens, gate_weight, up_weight, down_weight, in_gain, out_gain)
-    *flips, state = fused(tokens, gate_weight, up_weight, down_weight, in_gain, out_gain)
-    return tuple(emit(flips, state))
+    flips = fused(tokens, gate_weight, up_weight, down_weight, in_gain, out_gain)
+    return tuple(emit(flips, cols))
 
 
 def solution(mesh):

time: 289 us -> 209 us (0.72)
  Pallas kernels: 267 us -> 208 us
  local copies, waits for them, and re-layouts: 20.6 us -> 0 us
    pallas_call x1, Pallas kernels: 254 us -> 195 us  [fused(): pl.pallas_call(fused_kernel, in_specs=[whole] * 4 + [near] * 2, out_specs...]
    unnamed x16 -> x0, local copies, waits for them, and re-layouts: 20.6 us -> none
where the time goes in v2:
time: 209 us
  Pallas kernels  208 us (100%)
    pallas_call x1, Pallas kernels, fused(): pl.pallas_call(fused_kernel, in_specs=[whole] * 4 + [near] * 2, out_specs...  195 us
    pallas_call x1, Pallas kernels, emit(): pl.pallas_call(emit_kernel, in_specs=[near], out_specs=[whole] * 4, out_s...  12.9 us

profile of v2, /device:TPU:0, one launch (start us, length us, event | category | flops | bytes accessed | tf_op | source)
XLA Modules:
  0.0 209.1 jit_solution(3264943111186282583)
XLA Ops:
  0.6 195.4 %shard_map.93.flips = bf16[8576,2048]{1,0:T(8,128)(2,1)S(1)} custom-call(bf16[512,2048]{1,0:T(8,128)(2,1)} %tokens.1, f32[2,512,1408]{2,1,0:T(8,128)} %gate_w.1, f32[2,512,1408]{2,1,0:T(8,128)} %up_w.1, f32[2,512,1408]{2,1,0:T(8,128)} %down_w.1, f32[2,512]{1,0:T(2,128)} %in_gain.1, f32[2,2048]{1,0:T(2,128)} %out_gain.1), custom_call_target="tpu_custom_call" | custom-call | tf_op jit(solution)/shard_map/pallas_call | solution.py:604
  196.1 12.9 %shard_map.94 = (bf16[2,2048,1408]{2,1,0:T(8,128)(2,1)}, bf16[2,2048,1408]{2,1,0:T(8,128)(2,1)}, bf16[2,2048,1408]{2,1,0:T(8,128)(2,1)}, bf16[128,2048]{1,0:T(8,128)(2,1)}) custom-call(bf16[8576,2048]{1,0:T(8,128)(2,1)S(1)} %shard_map.93.flips), custom_call_target="tpu_custom_call" | custom-call | tf_op jit(solution)/shard_map/pallas_call | solution.py:676

commit v3 on v2

--- a/solution.py
+++ b/solution.py
@@ -97,8 +97,8 @@
     cols = gate_w.shape[2]
     full = [refs[0].at[pl.ds(m * cols, cols), :] for m in range(6)]
     state = refs[0]
-    stage, flip, tok, normed, hidden, part, rin, lin, rout, lout, rs_r, rs_l = refs[1:13]
-    load_sem, tok_sem, send_sem, recv_sem = refs[13:]
+    stage, flip, tok, normed, hidden, part, rin, lin, rout, lout, rs = refs[1:12]
+    load_sem, tok_sem, send_sem, recv_sem = refs[12:]
     y, z, t = lax.axis_index("grp"), lax.axis_index("fs"), lax.axis_index("tp")
     x, c = t // 2, lax.rem(t, 2)
     other_y, other_x, other_c = 1 - y, (1 - x) * 2 + c, x * 2 + (1 - c)
@@ -107,7 +107,6 @@
     ahead, behind = lax.rem(z + 1, groups), lax.rem(z + groups - 1, groups)
     to_x, to_c, to_y = {"tp": other_x}, {"tp": other_c}, {"grp": other_y}
     to_right, to_left = {"fs": ahead}, {"fs": behind}
-    inner = (z > 0) & (z < groups - 1)
     _, rows, cols = gate_w.shape
     half_rows = rows // 2
     block = cols // groups
@@ -194,12 +193,10 @@
     for partner in partners:
         pl.semaphore_signal(barrier, inc=1, device_id=partner, device_id_type=MESH)
 
-    z_sends = {}
-
     def prep(m):
         layer, which, s = m // 3, m % 3, m % 3
         if m >= 3:
-            for copy in z_sends[m - 3]:
+            for copy in copies_z(m - 3):
                 copy.wait_send()
         for r in range(2):
             k = 2 * m + r
@@ -221,24 +218,29 @@
         top = pl.multiple_of(t * block, 16)
         full[m][pl.ds(top, block), pl.ds(pl.multiple_of(z * rows, 128), rows)] = mine
 
-    def send_z(m):
-        z_sends[m] = []
+    def copies_z(m):
         base = [slot(("z", m, order)) for order in range(1, groups)][0]
         outer = 1 - (lax.rem(z, 3) + 1) // 2
+        copies = []
         for order in range(1, groups):
             target = origin(order)
             top = pl.multiple_of(target * block + y * half, 16)
             landing = base if order == 1 else base + 1 + outer
-            copy = pltpu.make_async_remote_copy(
-                src_ref=flip.at[m % 3, pl.ds(top, half), :],
-                dst_ref=place(m, t, y, z),
-                send_sem=send_sem.at[base + order - 1],
-                recv_sem=recv_sem.at[landing],
-                device_id={"fs": target},
-                device_id_type=MESH,
+            copies.append(
+                pltpu.make_async_remote_copy(
+                    src_ref=flip.at[m % 3, pl.ds(top, half), :],
+                    dst_ref=place(m, t, y, z),
+                    send_sem=send_sem.at[base + order - 1],
+                    recv_sem=recv_sem.at[landing],
+                    device_id={"fs": target},
+                    device_id_type=MESH,
+                )
             )
+        return copies
+
+    def send_z(m):
+        for copy in copies_z(m):
             copy.start()
-            z_sends[m].append(copy)
 
     def send_x(m):
         spot = blocks_of(m, t, z)
@@ -261,24 +263,30 @@
         arrived(("y", m, order), spot, to_y)
         sent.append(send(("w", m, order), spot, spot, to_x))
 
+    def share(m, far, order):
+        spot = blocks_of(m, other_x if far else t, origin(order) if order else z)
+        sent.append(send(("c", m, far, order), spot, spot, to_c))
+
     def finish(m):
+        share(m, 0, 0)
         arrived(("x", m, 0), blocks_of(m, other_x, z), to_x)
-        for shift in range(1, groups):
-            if (m, shift) in TURNED:
-                arrived(("x", m, shift), place(m, other_x, y, origin(shift)), to_x)
+        share(m, 1, 0)
+        for order in range(1, groups):
+            if (m, order) in TURNED:
+                arrived(("x", m, order), place(m, other_x, y, origin(order)), to_x)
             else:
-                arrived(("y", m, shift), place(m, t, other_y, origin(shift)), to_y)
-        mine = rows_of(m, t)
-        sent.append(send(("c", m, 0), mine, mine, to_c))
-        for shift in range(1, groups):
-            device = to_x if (m, shift) in TURNED else to_y
-            arrived(("w", m, shift), place(m, other_x, other_y, origin(shift)), device)
-        mine = rows_of(m, other_x)
-        sent.append(send(("c", m, 1), mine, mine, to_c))
+                arrived(("y", m, order), place(m, t, other_y, origin(order)), to_y)
+            share(m, 0, order)
+        for order in range(1, groups):
+            device = to_x if (m, order) in TURNED else to_y
+            arrived(("w", m, order), place(m, other_x, other_y, origin(order)), device)
+            share(m, 1, order)
 
     def on_c(m):
-        arrived(("c", m, 0), rows_of(m, other_c), to_c)
-        arrived(("c", m, 1), rows_of(m, other_both), to_c)
+        for far, column in ((0, other_c), (1, other_both)):
+            for order in range(groups):
+                spot = blocks_of(m, column, origin(order) if order else z)
+                arrived(("c", m, far, order), spot, to_c)
 
     def scaled(value):
         return value * lax.rsqrt(jnp.mean(value * value, axis=-1, keepdims=True) + EPS)
@@ -373,8 +381,8 @@
             near(i)
         if 0 <= i - 1 < 8:
             far(i - 1)
-        if 0 <= i - 2 < 8:
-            settle(i - 2)
+        if 0 <= i - 3 < 8:
+            settle(i - 3)
 
     def exchange_sent(first, last):
         for j in range(first, last):
@@ -394,77 +402,98 @@
         @pl.when(z == 0)
         def _():
             for j in parts_of(rightward):
-                send(("r", j), part.at[lines(j), :], rs_r.at[lines(j), :], to_right)
+                send(("r", j), part.at[lines(j), :], rs.at[lines(j), :], to_right)
 
         @pl.when(z == groups - 1)
         def _():
             for j in parts_of(leftward):
-                send(("l", j), part.at[lines(j), :], rs_l.at[lines(j), :], to_left)
+                send(("l", j), part.at[lines(j), :], rs.at[lines(j), :], to_left)
 
     def reduce_right(j):
-        arrived(("r", j), rs_r.at[lines(j), :], to_left)
-        add_into(rout, rs_r, None, j * piece, piece)
-        send(("r", j), rout.at[lines(j), :], rs_r.at[lines(j), :], to_right)
+        arrived(("r", j), rs.at[lines(j), :], to_left)
+        add_into(rout, rs, None, j * piece, piece)
+        send(("r", j), rout.at[lines(j), :], rs.at[lines(j), :], to_right)
 
     def reduce_left(j):
-        arrived(("l", j), rs_l.at[lines(j), :], to_right)
-        add_into(lout, rs_l, None, j * piece, piece)
-        send(("l", j), lout.at[lines(j), :], rs_l.at[lines(j), :], to_left)
+        arrived(("l", j), rs.at[lines(j), :], to_right)
+        add_into(lout, rs, None, j * piece, piece)
+        send(("l", j), lout.at[lines(j), :], rs.at[lines(j), :], to_left)
 
     def reduce_all():
-        zeros, ones, twos, threes = [parts_of(k) for k in range(groups)]
-
-        @pl.when(z == 1)
-        def _():
-            reduce_right(threes[0])
-            reduce_right(threes[1])
-            reduce_left(zeros[0])
-            reduce_right(twos[0])
-            reduce_left(zeros[1])
-            reduce_right(twos[1])
-
-        @pl.when(z == 2)
-        def _():
-            reduce_left(zeros[0])
-            reduce_left(zeros[1])
-            reduce_right(threes[0])
-            reduce_left(ones[0])
-            reduce_right(threes[1])
-            reduce_left(ones[1])
+        for j in range(2):
+
+            @pl.when(z == 1)
+            def _():
+                reduce_right(parts_of(3)[j])
+
+            @pl.when(z == 2)
+            def _():
+                reduce_left(parts_of(0)[j])
+
+    def leave(row, line, value):
+        state[pl.ds(line.start + row, 32), :] = value
 
     def conclude():
+        base = 6 * cols
         for k in range(groups):
-            for j in parts_of(k):
-
-                @pl.when(z == k)
+            start = ORDER.index(k) * quarter
+
+            @pl.when(z == k)
+            def _():
+                def keep(line):
+                    leave(base + 2 * quarter - start, line, part[line, :])
+                    leave(base + 3 * quarter - start, line, tok[line, :])
+
+                slabs(start, quarter, 32, keep)
+
+        for j in range(2):
+            for k in range(1, groups):
+                ahead_j = parts_of(k)[j]
+                shift = base - ORDER.index(k) * quarter
+
+                @pl.when(z == k - 1)
                 def _():
-                    if k > 0:
-                        arrived(("r", j), rs_r.at[lines(j), :], to_left)
-                    if k < groups - 1:
-                        arrived(("l", j), rs_l.at[lines(j), :], to_right)
-                    shift = 6 * cols - ORDER.index(k) * quarter
+                    if k > 1:
+                        arrived(("r", ahead_j), rs.at[lines(ahead_j), :], to_left)
 
                     def work(line):
                         total = part[line, :].astype(f32)
-                        if k > 0:
-                            total += rs_r[line, :].astype(f32)
-                        if k < groups - 1:
-                            total += rs_l[line, :].astype(f32)
-                        after = tok[line, :].astype(f32) + 0.5 * out_gain[1:2, :] * scaled(total)
-                        state[pl.ds(line.start + shift, 32), :] = after.astype(bf16)
-
-                    slabs(j * piece, piece, 32, work)
-
-        for k in range(groups):
+                        if k > 1:
+                            total += rs[line, :].astype(f32)
+                        leave(shift, line, total.astype(bf16))
+
+                    slabs(ahead_j * piece, piece, 32, work)
+
+            for k in reversed(range(groups - 1)):
+                back_j = parts_of(k)[j]
+                shift = base + quarter - ORDER.index(k) * quarter
+
+                @pl.when(z == k + 1)
+                def _():
+                    if k < groups - 2:
+                        arrived(("l", back_j), rs.at[lines(back_j), :], to_right)
+
+                    def work(line):
+                        total = part[line, :].astype(f32)
+                        if k < groups - 2:
+                            total += rs[line, :].astype(f32)
+                        leave(shift, line, total.astype(bf16))
+
+                    slabs(back_j * piece, piece, 32, work)
+
+        for k in (2, 3):
             for j in parts_of(k):
 
-                @pl.when(z < k)
+                @pl.when(z < k - 1)
                 def _():
-                    remote(("r", j), rout.at[lines(j), :], rs_r.at[lines(j), :], to_right).wait_send()
-
-                @pl.when(z > k)
+                    remote(("r", j), rout.at[lines(j), :], rs.at[lines(j), :], to_right).wait_send()
+
+        for k in (0, 1):
+            for j in parts_of(k):
+
+                @pl.when(z > k + 1)
                 def _():
-                    remote(("l", j), lout.at[lines(j), :], rs_l.at[lines(j), :], to_left).wait_send()
+                    remote(("l", j), lout.at[lines(j), :], rs.at[lines(j), :], to_left).wait_send()
 
     prep(0)
     pl.semaphore_wait(barrier, len(partners))
@@ -578,16 +607,16 @@
     summed(1, *upper)
     reduce_edge(3, 0)
     exchange(9)
+    exchange(10)
     for cut in pieces:
         gated(1, *lower, cut)
     exchange_sent(4, 8)
     summed(1, *lower)
     reduce_edge(2, 1)
-    reduce_edge(1, 2)
     reduce_all()
     conclude()
     for m in (3, 4, 5):
-        sent.extend(z_sends[m])
+        sent.extend(copies_z(m))
     for copy in sent:
         copy.wait_send()
 
@@ -600,12 +629,12 @@
     whole = pl.BlockSpec(memory_space=pl.ANY)
     near = pl.BlockSpec(memory_space=pltpu.VMEM)
     band = pltpu.VMEM((count, width), bf16)
-    messages = 128
+    messages = 160
     return pl.pallas_call(
         fused_kernel,
         in_specs=[whole] * 4 + [near] * 2,
         out_specs=near,
-        out_shape=pltpu.VMEM((6 * cols + quarter, width), bf16),
+        out_shape=pltpu.VMEM((6 * cols + count, width), bf16),
         scratch_shapes=[
             pltpu.VMEM((2, rows // 2, cols), jnp.float32),
             pltpu.VMEM((3, cols, rows), bf16),
@@ -618,27 +647,22 @@
             band,
             band,
             band,
-            band,
             pltpu.SemaphoreType.DMA((2,)),
             pltpu.SemaphoreType.DMA((4,)),
             pltpu.SemaphoreType.DMA((messages,)),
             pltpu.SemaphoreType.DMA((messages,)),
         ],
         compiler_params=pltpu.CompilerParams(
-            collective_id=0, has_side_effects=True, vmem_limit_bytes=29 * 2**20
+            collective_id=0, has_side_effects=True, vmem_limit_bytes=27 * 2**20
         ),
     )(tokens, gate_weight, up_weight, down_weight, in_gain, out_gain)
 
 
 def emit_kernel(flips, *refs):
-    outs, result = refs[:3], refs[3]
-    held, sems, state_sem = refs[4:]
+    outs, (held, sems) = refs[:3], refs[3:]
     slots, step, cols = held.shape
     width = flips.shape[1]
     steps = width // step
-    quarter = flips.shape[0] - 6 * cols
-    last = pltpu.make_async_copy(flips.at[pl.ds(6 * cols, quarter), :], result, state_sem)
-    last.start()
 
     def out_copy(k, i):
         slot = lax.rem(i, slots)
@@ -666,26 +690,52 @@
         lax.fori_loop(0, steps, one, 0)
     for i in range(slots):
         out_copy(5, steps - slots + i).wait()
-    last.wait()
 
 
 def emit(flips, cols):
-    height, width = flips.shape
+    width = flips.shape[1]
     near = pl.BlockSpec(memory_space=pltpu.VMEM)
     whole = pl.BlockSpec(memory_space=pl.ANY)
     return pl.pallas_call(
         emit_kernel,
         in_specs=[near],
-        out_specs=[whole] * 4,
-        out_shape=[jax.ShapeDtypeStruct((2, width, cols), jnp.bfloat16)] * 3
-        + [jax.ShapeDtypeStruct((height - 6 * cols, width), jnp.bfloat16)],
+        out_specs=[whole] * 3,
+        out_shape=[jax.ShapeDtypeStruct((2, width, cols), jnp.bfloat16)] * 3,
         scratch_shapes=[
             pltpu.VMEM((8, 256, cols), jnp.bfloat16),
             pltpu.SemaphoreType.DMA((8,)),
-            pltpu.SemaphoreType.DMA,
         ],
         compiler_params=pltpu.CompilerParams(vmem_limit_bytes=8 * 2**20),
+        cost_estimate=pl.CostEstimate(
+            flops=10**10, bytes_accessed=12 * cols * width, transcendentals=0
+        ),
     )(flips)
+
+
+def last_kernel(rest, left, right, out_gain, result):
+    quarter = result.shape[0]
+
+    def one(i, carry):
+        line = pl.ds(pl.multiple_of(i * 32, 32), 32)
+        total = rest[line, :].astype(jnp.float32) + left[line, :].astype(jnp.float32)
+        total += right[line, :].astype(jnp.float32)
+        before = rest[pl.ds(pl.multiple_of(quarter + i * 32, 32), 32), :].astype(jnp.float32)
+        after = before + 0.5 * out_gain[1:2, :] * normalize(total)
+        result[line, :] = after.astype(jnp.bfloat16)
+        return carry
+
+    lax.fori_loop(0, quarter // 32, one, 0)
+
+
+def last_step(rest, left, right, out_gain):
+    near = pl.BlockSpec(memory_space=pltpu.VMEM)
+    return pl.pallas_call(
+        last_kernel,
+        in_specs=[near] * 4,
+        out_specs=near,
+        out_shape=jax.ShapeDtypeStruct(left.shape, jnp.bfloat16),
+        compiler_params=pltpu.CompilerParams(vmem_limit_bytes=8 * 2**20),
+    )(rest, left, right, out_gain)
 
 
 def body(tokens, gate_weight, up_weight, down_weight, in_gain, out_gain):
@@ -697,7 +747,15 @@
     if odd or halves != 2 or columns != 4 or groups != 4:
         return body_plain(tokens, gate_weight, up_weight, down_weight, in_gain, out_gain)
     flips = fused(tokens, gate_weight, up_weight, down_weight, in_gain, out_gain)
-    return tuple(emit(flips, cols))
+    quarter = count // groups
+    base = 6 * cols
+    ahead = lax.slice_in_dim(flips, base, base + quarter)
+    back = lax.slice_in_dim(flips, base + quarter, base + 2 * quarter)
+    rest = lax.slice_in_dim(flips, base + 2 * quarter, base + 4 * quarter)
+    left = lax.ppermute(ahead, "fs", [(i, i + 1) for i in range(groups - 1)])
+    right = lax.ppermute(back, "fs", [(i + 1, i) for i in range(groups - 1)])
+    outs = emit(flips, cols)
+    return (*outs, last_step(rest, left, right, out_gain))
 
 
 def solution(mesh):

time: 209 us -> 202 us (0.967)
  Pallas kernels: 208 us -> 193 us
  starting transfers between devices: 0 us -> 5.87 us
    pallas_call x1, Pallas kernels: 195 us -> 179 us  [fused(): pl.pallas_call(fused_kernel, in_specs=[whole] * 4 + [near] * 2, out_specs...]
    ppermute x0 -> x2, starting transfers between devices: none -> 5.87 us  [the longest x1 4.57 us: body(): left = lax.ppermute(ahead, 'fs', [(i, i + 1) for i in range(groups - 1)])]
    pallas_call x1 -> x2, Pallas kernels: 12.9 us -> 14.3 us  [the longest x1 12.9 us: emit(): pl.pallas_call(emit_kernel, in_specs=[near], out_specs=[whole] * 3, out_s...]
  transfers between devices with their start and end apart: 0 -> 2, of which waited for: 0 -> 1; matrix products, arithmetic and copies ran while one was open for 0% -> 0% of each run, Pallas kernels for 0% -> 6%
where the time goes in v3:
time: 202 us; the launch traced here: 201 us
  Pallas kernels  193 us (96%)
  starting transfers between devices  5.87 us (3%)
    pallas_call x1, Pallas kernels, fused(): pl.pallas_call(fused_kernel, in_specs=[whole] * 4 + [near] * 2, out_specs...  179 us
    pallas_call x1, Pallas kernels, emit(): pl.pallas_call(emit_kernel, in_specs=[near], out_specs=[whole] * 3, out_s...  12.9 us
    ppermute x1, starting transfers between devices, body(): left = lax.ppermute(ahead, 'fs', [(i, i + 1) for i in range(groups - 1)])  4.57 us
  transfers between devices with their start and end apart: 2, of which 1 were waited for; matrix products, arithmetic and copies ran while one was open for 0% of the time, Pallas kernels for 6%

profile of v3, /device:TPU:0, one launch (start us, length us, event | category | flops | bytes accessed | tf_op | source)
XLA Modules:
  0.0 201.5 jit_solution(14234529018630920700)
XLA Ops:
  0.6 178.8 %shard_map.93.flips = bf16[8960,2048]{1,0:T(8,128)(2,1)S(1)} custom-call(bf16[512,2048]{1,0:T(8,128)(2,1)} %tokens.1, f32[2,512,1408]{2,1,0:T(8,128)} %gate_w.1, f32[2,512,1408]{2,1,0:T(8,128)} %up_w.1, f32[2,512,1408]{2,1,0:T(8,128)} %down_w.1, f32[2,512]{1,0:T(2,128)} %in_gain.1, f32[2,2048]{1,0:T(2,128)} %out_gain.3), custom_call_target="tpu_custom_call" | custom-call | tf_op jit(solution)/shard_map/pallas_call | solution.py:633
  179.4 0.1 fusion
  179.5 4.6 %collective-permute-start = (bf16[128,2048]{1,0:T(8,128)(2,1)S(1)}, bf16[128,2048]{1,0:T(8,128)(2,1)S(1)}, u32[]{:S(2)}, u32[]{:S(2)}) collective-permute-start(bf16[128,2048]{1,0:T(8,128)(2,1)S(1)} %get-tuple-element.11), channel_id=1, source_target_pairs={{0,4},{4,8},{8,12},{1,5},{5,9},{9,13},{2,6},{6,10},{10,14},{3,7},{... | collective-permute-start | bytes 1572872 | tf_op jit(solution)/shard_map/ppermute | solution.py:755
  184.1 1.3 collective-permute-start.1
  185.4 0.1 slice.9.rest
  185.5 0.0 copy-start
  185.5 12.9 %shard_map.94 = (bf16[2,2048,1408]{2,1,0:T(8,128)(2,1)}, bf16[2,2048,1408]{2,1,0:T(8,128)(2,1)}, bf16[2,2048,1408]{2,1,0:T(8,128)(2,1)}) custom-call(bf16[8960,2048]{1,0:T(8,128)(2,1)S(1)} %shard_map.93.flips), custom_call_target="tpu_custom_call" | custom-call | flops 10000000000 | bytes 34603008 | tf_op jit(solution)/shard_map/pallas_call | solution.py:699
  198.3 0.0 collective-permute-done.left
  198.3 1.6 collective-permute-done.1.right
  200.0 0.0 copy-done
  200.0 1.5 shard_map.95
Async XLA Ops:
  179.5 18.8 %collective-permute-start = (bf16[128,2048]{1,0:T(8,128)(2,1)S(1)}, bf16[128,2048]{1,0:T(8,128)(2,1)S(1)}, u32[]{:S(2)}, u32[]{:S(2)}) collective-permute-start(bf16[128,2048]{1,0:T(8,128)(2,1)S(1)} %get-tuple-element.11), channel_id=1, source_target_pairs={{0,4},{4,8},{8,12},{1,5},{5,9},{9,13},{2,6},{6,10},{10,14},{3,7},{... | collective-permute-start | bytes 1572872 | tf_op jit(solution)/shard_map/ppermute | solution.py:755
  184.1 15.9 %collective-permute-start.1 = (bf16[128,2048]{1,0:T(8,128)(2,1)S(1)}, bf16[128,2048]{1,0:T(8,128)(2,1)S(1)}, u32[]{:S(2)}, u32[]{:S(2)}) collective-permute-start(bf16[128,2048]{1,0:T(8,128)(2,1)S(1)} %get-tuple-element.10), channel_id=1, source_target_pairs={{4,0},{8,4},{12,8},{5,1},{9,5},{13,9},{6,2},{10,6},{14,10},{7,3},{... | collective-permute-start | bytes 1572872 | tf_op jit(solution)/shard_map/ppermute | solution.py:756
  185.5 14.5 %copy-start = (f32[2,2048]{1,0:T(2,128)S(1)}, f32[2,2048]{1,0:T(2,128)}, u32[]{:S(2)}) copy-start(f32[2,2048]{1,0:T(2,128)} %out_gain.3) | copy-start | bytes 49156

commit v4 on v3

--- a/solution.py
+++ b/solution.py
@@ -184,8 +184,6 @@
         )
     load(0).start()
     load(1).start()
-    for copy in fetch:
-        copy.start()
 
     partners = [{"fs": lax.rem(z + shift, groups)} for shift in range(1, groups)]
     partners += [to_x, to_c, to_y]
@@ -193,10 +191,10 @@
     for partner in partners:
         pl.semaphore_signal(barrier, inc=1, device_id=partner, device_id_type=MESH)
 
-    def prep(m):
+    def prep(m, after=None):
         layer, which, s = m // 3, m % 3, m % 3
         if m >= 3:
-            for copy in copies_z(m - 3):
+            for copy in all_z(m - 3):
                 copy.wait_send()
         for r in range(2):
             k = 2 * m + r
@@ -212,24 +210,30 @@
                 return carry
 
             lax.fori_loop(0, cols // 128, one, 0)
+            if after is not None:
+                after(r)
             if k + 2 < 12:
                 load(k + 2).start()
         mine = flip[s, pl.ds(pl.multiple_of(z * block, 16), block), :]
         top = pl.multiple_of(t * block, 16)
         full[m][pl.ds(top, block), pl.ds(pl.multiple_of(z * rows, 128), rows)] = mine
 
-    def copies_z(m):
-        base = [slot(("z", m, order)) for order in range(1, groups)][0]
-        outer = 1 - (lax.rem(z, 3) + 1) // 2
+    def copies_z(m, part_of=None):
+        kind = "z" if part_of is None else ("z0", "z1")[part_of]
+        base = [slot((kind, m, order)) for order in range(1, groups)][0]
+        first, size = (0, rows) if part_of is None else (part_of * half_rows, half_rows)
+        lanes = pl.ds(pl.multiple_of(z * rows + first, 128), size)
+        spot = full[m].at[pl.ds(pl.multiple_of(t * block + y * half, 16), half), lanes]
+        late = 1 - (lax.rem(z, 3) + 1) // 2
         copies = []
         for order in range(1, groups):
             target = origin(order)
             top = pl.multiple_of(target * block + y * half, 16)
-            landing = base if order == 1 else base + 1 + outer
+            landing = base if order == 1 else base + 1 + late
             copies.append(
                 pltpu.make_async_remote_copy(
-                    src_ref=flip.at[m % 3, pl.ds(top, half), :],
-                    dst_ref=place(m, t, y, z),
+                    src_ref=flip.at[m % 3, pl.ds(top, half), pl.ds(first, size)],
+                    dst_ref=spot,
                     send_sem=send_sem.at[base + order - 1],
                     recv_sem=recv_sem.at[landing],
                     device_id={"fs": target},
@@ -238,18 +242,32 @@
             )
         return copies
 
+    def all_z(m):
+        return copies_z(0, 0) + copies_z(0, 1) if m == 0 else copies_z(m)
+
     def send_z(m):
         for copy in copies_z(m):
             copy.start()
 
+    def own_x(m):
+        spot = blocks_of(m, t, z)
+        return remote(("x", m, 0), spot, spot, to_x)
+
     def send_x(m):
-        spot = blocks_of(m, t, z)
-        sent.append(send(("x", m, 0), spot, spot, to_x))
+        own_x(m).start()
+        sent.append(own_x(m))
 
     def on_z(m, shift):
         source = origin(shift)
         spot = place(m, t, y, source)
-        arrived(("z", m, shift), spot, {"fs": source})
+        if m == 0:
+            top = pl.multiple_of(t * block + y * half, 16)
+            for r in range(2):
+                lanes = pl.ds(pl.multiple_of(source * rows + r * half_rows, 128), half_rows)
+                landed = full[m].at[pl.ds(top, half), lanes]
+                arrived((("z0", "z1")[r], m, shift), landed, {"fs": source})
+        else:
+            arrived(("z", m, shift), spot, {"fs": source})
         sent.append(send(("x", m, shift), spot, spot, to_x))
         sent.append(send(("y", m, shift), spot, spot, to_y))
 
@@ -495,10 +513,16 @@
                 def _():
                     remote(("l", j), lout.at[lines(j), :], rs.at[lines(j), :], to_left).wait_send()
 
-    prep(0)
-    pl.semaphore_wait(barrier, len(partners))
-    send_z(0)
+    def early(r):
+        if r == 0:
+            pl.semaphore_wait(barrier, len(partners))
+        for copy in copies_z(0, r):
+            copy.start()
+
+    prep(0, early)
     send_x(0)
+    for copy in fetch:
+        copy.start()
     prep(1)
     prep(2)
     for copy in fetch:
@@ -559,10 +583,9 @@
     gated(0, *whole, pieces[1])
     on_z(3, 3)
     gated(0, *whole, pieces[2])
-    on_x(3, 1)
     gated(0, *whole, pieces[3])
     finish(2)
-    on_x(3, 2)
+    on_x(3, 1)
     send_x(3)
     on_c(2)
     summed(0, *upper)
@@ -571,26 +594,27 @@
     summed(0, *lower)
     for j in range(4, 8):
         edge(j)
-    on_x(3, 3)
+    on_x(3, 2)
     on_z(4, 1)
     on_z(4, 2)
+    on_x(3, 3)
     on_z(4, 3)
+    send_x(4)
     exchange(0)
-    finish(3)
     exchange(1)
     turn(4, 1)
     on_x(4, 2)
     exchange(2)
-    on_x(4, 3)
-    send_x(4)
     on_z(5, 1)
     on_z(5, 2)
+    on_x(4, 3)
+    on_z(5, 3)
+    send_x(5)
     exchange(3)
+    finish(3)
+    exchange(4)
     on_x(5, 1)
-    on_z(5, 3)
-    exchange(4)
     finish(4)
-    send_x(5)
     exchange(5)
     on_x(5, 2)
     exchange(6)

time: 202 us -> 199 us (0.985)
  no operation moved by 1% of the time
where the time goes in v4:
time: 199 us
  Pallas kernels  192 us (96%)
  starting transfers between devices  5.87 us (3%)
    pallas_call x1, Pallas kernels, fused(): pl.pallas_call(fused_kernel, in_specs=[whole] * 4 + [near] * 2, out_specs...  178 us
    pallas_call x1, Pallas kernels, emit(): pl.pallas_call(emit_kernel, in_specs=[near], out_specs=[whole] * 3, out_s...  12.9 us
    ppermute x1, starting transfers between devices, body(): left = lax.ppermute(ahead, 'fs', [(i, i + 1) for i in range(groups - 1)])  4.57 us
  transfers between devices with their start and end apart: 2, of which 1 were waited for; matrix products, arithmetic and copies ran while one was open for 0% of the time, Pallas kernels for 6%

profile of v4, /device:TPU:0, one launch (start us, length us, event | category | flops | bytes accessed | tf_op | source)
XLA Modules:
  0.0 199.0 jit_solution(646141766499748795)
XLA Ops:
  0.6 177.9 %shard_map.93.flips = bf16[8960,2048]{1,0:T(8,128)(2,1)S(1)} custom-call(bf16[512,2048]{1,0:T(8,128)(2,1)} %tokens.1, f32[2,512,1408]{2,1,0:T(8,128)} %gate_w.1, f32[2,512,1408]{2,1,0:T(8,128)} %up_w.1, f32[2,512,1408]{2,1,0:T(8,128)} %down_w.1, f32[2,512]{1,0:T(2,128)} %in_gain.1, f32[2,2048]{1,0:T(2,128)} %out_gain.3), custom_call_target="tpu_custom_call" | custom-call | tf_op jit(solution)/shard_map/pallas_call | solution.py:657
  178.5 0.1 fusion
  178.6 4.6 %collective-permute-start = (bf16[128,2048]{1,0:T(8,128)(2,1)S(1)}, bf16[128,2048]{1,0:T(8,128)(2,1)S(1)}, u32[]{:S(2)}, u32[]{:S(2)}) collective-permute-start(bf16[128,2048]{1,0:T(8,128)(2,1)S(1)} %get-tuple-element.11), channel_id=1, source_target_pairs={{0,4},{4,8},{8,12},{1,5},{5,9},{9,13},{2,6},{6,10},{10,14},{3,7},{... | collective-permute-start | bytes 1572872 | tf_op jit(solution)/shard_map/ppermute | solution.py:779
  183.2 1.3 collective-permute-start.1
  184.5 0.1 slice.9.rest
  184.6 0.0 copy-start
  184.6 12.9 %shard_map.94 = (bf16[2,2048,1408]{2,1,0:T(8,128)(2,1)}, bf16[2,2048,1408]{2,1,0:T(8,128)(2,1)}, bf16[2,2048,1408]{2,1,0:T(8,128)(2,1)}) custom-call(bf16[8960,2048]{1,0:T(8,128)(2,1)S(1)} %shard_map.93.flips), custom_call_target="tpu_custom_call" | custom-call | flops 10000000000 | bytes 34603008 | tf_op jit(solution)/shard_map/pallas_call | solution.py:723
  197.4 0.0 collective-permute-done.left
  197.4 0.1 collective-permute-done.1.right
  197.6 0.0 copy-done
  197.6 1.5 shard_map.95
Async XLA Ops:
  178.6 18.8 %collective-permute-start = (bf16[128,2048]{1,0:T(8,128)(2,1)S(1)}, bf16[128,2048]{1,0:T(8,128)(2,1)S(1)}, u32[]{:S(2)}, u32[]{:S(2)}) collective-permute-start(bf16[128,2048]{1,0:T(8,128)(2,1)S(1)} %get-tuple-element.11), channel_id=1, source_target_pairs={{0,4},{4,8},{8,12},{1,5},{5,9},{9,13},{2,6},{6,10},{10,14},{3,7},{... | collective-permute-start | bytes 1572872 | tf_op jit(solution)/shard_map/ppermute | solution.py:779
  183.2 14.4 %collective-permute-start.1 = (bf16[128,2048]{1,0:T(8,128)(2,1)S(1)}, bf16[128,2048]{1,0:T(8,128)(2,1)S(1)}, u32[]{:S(2)}, u32[]{:S(2)}) collective-permute-start(bf16[128,2048]{1,0:T(8,128)(2,1)S(1)} %get-tuple-element.10), channel_id=1, source_target_pairs={{4,0},{8,4},{12,8},{5,1},{9,5},{13,9},{6,2},{10,6},{14,10},{7,3},{... | collective-permute-start | bytes 1572872 | tf_op jit(solution)/shard_map/ppermute | solution.py:780
  184.6 13.0 %copy-start = (f32[2,2048]{1,0:T(2,128)S(1)}, f32[2,2048]{1,0:T(2,128)}, u32[]{:S(2)}) copy-start(f32[2,2048]{1,0:T(2,128)} %out_gain.3) | copy-start | bytes 49156
